TPU v7x, 32 devices: a whole 2x2x4 slice. The times are simulated.
32 devices in a mesh: fs: 8 (over z, x), tp: 4 (over y, core).
Axes of the slice: x: 2, y: 2, z: 4, core: 2. Of those that a mesh axis runs over, the one named last changes fastest.
Arguments:
- later_rows: bfloat16 [4096, 2048], P(('fs', 'tp')), may hold values from -6 to 6
- earlier_rows: bfloat16 [4096, 2048], P(('fs', 'tp')), may hold values from -6 to 6
- cotangent: bfloat16 [4096, 2048], P(('fs', 'tp')), may hold values from -6 to 6
- up_weight: bfloat16 [2048, 4096], P('fs', 'tp'), may hold values from -0.125 to 0.125
- down_weight: bfloat16 [2048, 4096], P('fs', 'tp'), may hold values from -0.09375 to 0.09375
- up_total: float32 [2048, 4096], P('fs', 'tp'), may hold values from -6 to 6
- down_total: float32 [2048, 4096], P('fs', 'tp'), may hold values from -6 to 6
Outputs:
- later_out: bfloat16 [4096, 2048], P(('fs', 'tp'))
- earlier_grad: bfloat16 [4096, 2048], P(('fs', 'tp'))
- up_updated: float32 [2048, 4096], P('fs', 'tp')
- down_updated: float32 [2048, 4096], P('fs', 'tp')
All inputs are finite; a program needn't handle non-finite values.
Results may differ from a plain program's by a relative error of at most 0.015.
Values may be sent and summed in bfloat16 or wider, within the bound.
A program may use at most 128 MiB of HBM per device.

v0:
```python
import functools
import math

import jax
import jax.numpy as jnp
from jax import lax
from jax.experimental import pallas as pl
from jax.experimental.pallas import tpu as pltpu
from jax.sharding import PartitionSpec as P

MESH = pl.DeviceIdType.MESH
BF16 = jnp.bfloat16
F32 = jnp.float32


def columns_of(n):
    best = 1
    for x in range(1, n + 1):
        if n % x == 0 and 2 * x * x <= n and (n // x) % 2 == 0:
            best = x
    return best


def ring_to_fs(p, n, x_size):
    if x_size == 1:
        return p
    z_size, wide = n // x_size, x_size - 1
    body = z_size * wide
    z, r = p // wide, p % wide
    x = 1 + jnp.where(z % 2 == 0, r, wide - 1 - r)
    back = z_size - 1 - (p - body)
    return jnp.where(p < body, z * x_size + x, back * x_size)


def fs_to_ring(f, n, x_size):
    if x_size == 1:
        return f
    z_size, wide = n // x_size, x_size - 1
    z, x = f // x_size, f % x_size
    r = jnp.where(z % 2 == 0, x - 1, x_size - 1 - x)
    return jnp.where(x == 0, z_size * wide + z_size - 1 - z, z * wide + r)


def kernel(n, m, parts,
           later_ref, earlier_ref, cot_ref, up_ref, down_ref,
           later_out, earlier_out, up_out, down_out,
           tok, wts, acc, hid, grads, rbuf, part, dbuf, ybuf,
           ty_s, ty_r, td_s, td_r, w_s, w_r, g_s, g_r, od_s, od_r, oy_s, oy_r):
    rows_dev, depth = later_ref.shape
    blk, width = up_ref.shape
    rows = rows_dev * m
    half, y_size = n // 2, m // 2
    aligned = blk % 128 == 0
    wide_q = width // parts
    fs, tp = lax.axis_index("fs"), lax.axis_index("tp")
    x_size = columns_of(n)
    pos = fs_to_ring(fs, n, x_size)
    y, c = tp // 2, tp % 2

    def at_ring(p):
        return ring_to_fs((p + 2 * n) % n, n, x_size)

    right = {"fs": at_ring(pos + 1), "tp": tp}
    left = {"fs": at_ring(pos - 1), "tp": tp}
    mate = {"fs": fs, "tp": y * 2 + 1 - c}
    y_next = {"fs": fs, "tp": ((y + 1) % y_size) * 2 + c}
    y_prev = {"fs": fs, "tp": ((y + y_size - 1) % y_size) * 2 + c}

    barrier = pltpu.get_barrier_semaphore()
    for other in (right, left, mate, y_next, y_prev):
        pl.semaphore_signal(barrier, inc=1, device_id=other, device_id_type=MESH)
    pl.semaphore_wait(barrier, 5)

    def remote(src, dst, send, recv, to):
        return pltpu.make_async_remote_copy(
            src_ref=src, dst_ref=dst, send_sem=send, recv_sem=recv, device_id=to, device_id_type=MESH)

    def trows(a, t):
        return tok.at[a, pl.ds(pl.multiple_of(t * rows_dev, rows_dev), rows_dev), :]

    own_w, own_t = (up_ref, down_ref), (earlier_ref, cot_ref, later_ref)

    arr_of, sign_of = (0, 1, 1, 0), (1, -1, 1, -1)

    def cut(q):
        return pl.ds(q * wide_q, wide_q)

    def w_copy(k, s, q, first=False):
        f = at_ring(pos - sign_of[k] * s)
        there = wts.at[arr_of[k], pl.ds(pl.multiple_of(f * blk, blk), blk), cut(q)]
        src = own_w[arr_of[k]].at[:, cut(q)] if first else there
        return remote(src, there, w_s.at[k, s, q], w_r.at[k, s, q], right if sign_of[k] > 0 else left)

    def ty_copy(a, s, first=False):
        t = ((y + y_size - s) % y_size) * 2 + c
        return remote(own_t[a] if first else trows(a, t), trows(a, t), ty_s.at[a, s], ty_r.at[a, s], y_next)

    def td_copy(a, s, first=False):
        t = ((y + y_size - s) % y_size) * 2 + c
        return remote(own_t[a] if first else trows(a, t), trows(a, t), td_s.at[a, s], td_r.at[a, s], mate)

    every = tuple((k, q) for pair in ((0, 1), (2, 3)) for q in range(parts) for k in pair)
    longs = tuple((k, q) for k, q in every if k < 2)
    for k, q in every:
        w_copy(k, 0, q, True).start()
    for a in range(3):
        if y_size > 1:
            ty_copy(a, 0, True).start()
    for a in range(3):
        td_copy(a, 0, True).start()

    def put(dst, dst_row, src, count):
        step = math.gcd(count, 64)

        @pl.loop(0, count // step)
        def _(i):
            o = pl.multiple_of(i * step, step)
            dst[pl.ds(pl.multiple_of(dst_row + o, step), step), :] = src[pl.ds(o, step), :]

    for a in range(2):
        put(wts.at[a], fs * blk, own_w[a], blk)
    for a in range(3):
        put(tok.at[a], tp * rows_dev, own_t[a], rows_dev)

    tile = math.gcd(wide_q, 256)

    def multiply(a, w, rows_w, clear, q=None):
        first, count = (0, width) if q is None else (q * wide_q, wide_q)

        @pl.loop(0, count // tile)
        def _(j):
            o = pl.ds(pl.multiple_of(first + j * tile, tile), tile)
            got = jnp.dot(tok[a, :, rows_w], wts[w, rows_w, o], preferred_element_type=F32)
            if clear:
                acc[a, :, o] = got
            else:
                acc[a, :, o] += got

    def use(w, f, clear=False, q=None):
        if not aligned:
            return
        o = pl.ds(pl.multiple_of(f * blk, blk), blk)
        for a in ((0, 2) if w == 0 else (1,)):
            multiply(a, w, o, clear, q)

    def forward(s, present, go):
        for k, q in present:
            w_copy(k, s - 1, q).wait_recv()
            if (k, q) in go:
                w_copy(k, s, q).start()

    def use_step(s):
        for k in range(4):
            use(arr_of[k], at_ring(pos - sign_of[k] * s))

    forward(1, every, every if half > 2 else longs)
    for s in range(1, y_size):
        for a in range(3):
            ty_copy(a, s - 1).wait_recv()
            if s < y_size - 1:
                ty_copy(a, s).start()
            td_copy(a, s).start()
    for s in range(y_size):
        for a in range(3):
            td_copy(a, s).wait_recv()
    for w in range(2):
        use(w, fs, True)
    if half > 3:
        @pl.loop(2, half - 1)
        def _(s):
            forward(s, every, every)
            use_step(s - 1)
    if half > 2:
        forward(half - 1, every, longs)
        use_step(half - 2)
    use_step(half - 1)

    step_r = math.gcd(rows, 32)

    def activate(q):
        @pl.loop(0, rows // step_r)
        def _(i):
            o = pl.ds(pl.multiple_of(i * step_r, step_r), step_r)
            relu = jnp.maximum(acc[0, o, cut(q)], 0.0)
            hid[0, o, cut(q)] = (2.0 * relu * acc[1, o, cut(q)]).astype(BF16)
            hid[1, o, cut(q)] = (relu * relu).astype(BF16)

    def term(a, row, size, q=None):
        first, count = (0, width) if q is None else (q * wide_q, wide_q)

        @pl.loop(0, count // tile)
        def _(j):
            o = pl.ds(pl.multiple_of(first + j * tile, tile), tile)
            grads[a, pl.ds(row, size), o] = lax.dot_general(
                tok[a, :, pl.ds(row, size)], hid[a, :, o], (((0,), (0,)), ((), ())),
                preferred_element_type=F32).astype(BF16)

    def block_term(a, p, q=None):
        term(a, pl.multiple_of(at_ring(p) * blk, blk), blk, q)

    def g_copy(k, s, q):
        d = half - (k >= 2) - s
        f = at_ring(pos + sign_of[k] * d)
        src = grads.at[arr_of[k], pl.ds(pl.multiple_of(f * blk, blk), blk), cut(q)]
        return remote(src, rbuf.at[k, s, :, cut(q)], g_s.at[k, s, q], g_r.at[k, s, q],
                      right if sign_of[k] > 0 else left)

    def add_rows(dst, dst_row, src, count, columns=slice(None)):
        step = math.gcd(count, 32)

        @pl.loop(0, count // step)
        def _(i):
            o = pl.multiple_of(i * step, step)
            at = pl.ds(pl.multiple_of(dst_row + o, step), step)
            total = dst[at, columns].astype(F32) + src[pl.ds(o, step), columns].astype(F32)
            dst[at, columns] = total.astype(BF16)

    def g_step(s, which):
        for k, q in which:
            g_copy(k, s - 1, q).wait_recv()
            f = at_ring(pos + sign_of[k] * (half - (k >= 2) - s))
            add_rows(grads.at[arr_of[k]], f * blk, rbuf.at[k, s - 1], blk, cut(q))
            g_copy(k, s, q).start()

    wide = math.gcd(depth, 256)
    for q in range(parts):
        for k in (0, 1):
            w_copy(k, half - 1, q).wait_recv()
            use(arr_of[k], at_ring(pos - sign_of[k] * half), q=q)
        if not aligned:
            full = pl.ds(0, depth)
            for a, w in ((0, 0), (1, 1), (2, 0)):
                multiply(a, w, full, True, q)
        activate(q)
        if not aligned:
            for a in range(2):
                @pl.loop(0, depth // wide)
                def _(i):
                    term(a, pl.multiple_of(i * wide, wide), wide, q)
        for k in (0, 1):
            if aligned:
                block_term(arr_of[k], pos + sign_of[k] * half, q)
            g_copy(k, 0, q).start()
    for k in (2, 3):
        if aligned:
            block_term(arr_of[k], pos + sign_of[k] * (half - 1))
        for q in range(parts):
            g_copy(k, 0, q).start()
    if aligned:
        if half > 1:
            @pl.loop(0, half - 1)
            def _(i):
                d = half - 1 - i
                block_term(0, pos + d)
                block_term(1, pos - d)
        if half > 2:
            @pl.loop(0, half - 2)
            def _(i):
                d = half - 2 - i
                block_term(1, pos + d)
                block_term(0, pos - d)
        for a in range(2):
            block_term(a, pos)

    @pl.loop(0, rows // step_r)
    def _(i):
        o = pl.ds(pl.multiple_of(i * step_r, step_r), step_r)
        relu = jnp.maximum(acc[2, o, :], 0.0)
        hid[2, o, :] = (relu * relu).astype(BF16)

    wide_d = math.gcd(depth, 256)

    def partial(a, h, w):
        @pl.loop(0, depth // wide_d)
        def _(j):
            o = pl.ds(pl.multiple_of(j * wide_d, wide_d), wide_d)
            part[a, :, o] = lax.dot_general(
                hid[h], wts[w, o, :], (((1,), (1,)), ((), ())), preferred_element_type=F32).astype(BF16)

    def prow(yy, cc):
        return pl.multiple_of((yy * 2 + cc) * rows_dev, rows_dev)

    def od_copy(a, yy):
        return remote(part.at[a, pl.ds(prow(yy, 1 - c), rows_dev), :], dbuf.at[a, yy],
                      od_s.at[a, yy], od_r.at[a, yy], mate)

    def oy_copy(a, s):
        t = (y + y_size - 1 - s) % y_size
        return remote(part.at[a, pl.ds(prow(t, c), rows_dev), :], ybuf.at[a, s],
                      oy_s.at[a, s], oy_r.at[a, s], y_next)

    def send_partial(a, h, w):
        partial(a, h, w)
        for yy in range(y_size):
            od_copy(a, yy).start()

    send_partial(0, 0, 0)
    g_step(1, every if half > 2 else longs)
    send_partial(1, 2, 1)
    for a in range(2):
        for yy in range(y_size):
            od_copy(a, yy).wait_recv()
            add_rows(part.at[a], prow(yy, c), dbuf.at[a, yy], rows_dev)
        if y_size > 1:
            oy_copy(a, 0).start()
    if half - 1 > 2:
        @pl.loop(2, half - 1)
        def _(s):
            g_step(s, every)
    for s in range(1, y_size):
        for a in range(2):
            oy_copy(a, s - 1).wait_recv()
            t = (y + y_size - 1 - s) % y_size
            add_rows(part.at[a], prow(t, c), ybuf.at[a, s - 1], rows_dev)
            if s < y_size - 1:
                oy_copy(a, s).start()
    put_own = ((earlier_out, 0), (later_out, 1))
    for out, a in put_own:
        out[...] = part[a, pl.ds(prow(y, c), rows_dev), :]
    if half - 1 >= 2:
        g_step(half - 1, longs)

    ends = [(k, half - 1 - (k >= 2)) for k in range(4)]
    for k, q in tuple((k, q) for k, q in every if k >= 2) + longs:
        g_copy(k, ends[k][1], q).wait_recv()
    step_b = math.gcd(blk, 32)
    for a, out in ((0, up_out), (1, down_out)):
        @pl.loop(0, blk // step_b)
        def _(i):
            lo = pl.multiple_of(i * step_b, step_b)
            o = pl.ds(lo, step_b)
            got = grads[a, pl.ds(pl.multiple_of(fs * blk + lo, step_b), step_b), :].astype(F32)
            for k, s in ends:
                if arr_of[k] == a:
                    got += rbuf[k, s, o, :].astype(F32)
            out[o, :] = got.astype(BF16)

    for k, q in every:
        for s in range(half - (k >= 2)):
            w_copy(k, s, q).wait_send()
            g_copy(k, s, q).wait_send()
    for a in range(3):
        for s in range(y_size):
            if s < y_size - 1:
                ty_copy(a, s).wait_send()
            td_copy(a, s).wait_send()
    for a in range(2):
        for yy in range(y_size):
            od_copy(a, yy).wait_send()
        for s in range(y_size - 1):
            oy_copy(a, s).wait_send()


def body(n, m, later_rows, earlier_rows, cotangent, up_weight, down_weight, up_total, down_total):
    rows_dev, depth = later_rows.shape
    blk, width = up_weight.shape
    rows, half, y_size = rows_dev * m, n // 2, m // 2
    factor = 1.0 / math.sqrt(rows * n)
    dma = pltpu.SemaphoreType.DMA
    vmem = pl.BlockSpec(memory_space=pltpu.VMEM)
    sums = max(y_size - 1, 1)
    parts = 2 if width % 256 == 0 else 1
    later_out, earlier_grad, up_term, down_term = pl.pallas_call(
        functools.partial(kernel, n, m, parts),
        out_shape=(
            jax.ShapeDtypeStruct((rows_dev, depth), BF16),
            jax.ShapeDtypeStruct((rows_dev, depth), BF16),
            jax.ShapeDtypeStruct((blk, width), BF16),
            jax.ShapeDtypeStruct((blk, width), BF16),
        ),
        in_specs=[vmem] * 5,
        out_specs=(vmem,) * 4,
        scratch_shapes=[
            pltpu.VMEM((3, rows, depth), BF16),
            pltpu.VMEM((2, depth, width), BF16),
            pltpu.VMEM((3, rows, width), F32),
            pltpu.VMEM((3, rows, width), BF16),
            pltpu.VMEM((2, depth, width), BF16),
            pltpu.VMEM((4, half, blk, width), BF16),
            pltpu.VMEM((2, rows, depth), BF16),
            pltpu.VMEM((2, y_size, rows_dev, depth), BF16),
            pltpu.VMEM((2, sums, rows_dev, depth), BF16),
            dma((3, y_size)), dma((3, y_size)), dma((3, y_size)), dma((3, y_size)),
            *[dma((4, half, parts))] * 4,
            dma((2, y_size)), dma((2, y_size)), dma((2, sums)), dma((2, sums)),
        ],
        compiler_params=pltpu.CompilerParams(
            collective_id=0, has_side_effects=True, vmem_limit_bytes=67043328
        ),
        name="feed_forward_step",
    )(later_rows, earlier_rows, cotangent, up_weight, down_weight)
    up_updated = up_total + up_term.astype(F32) * factor
    down_updated = down_total + down_term.astype(F32) * factor
    return later_out, earlier_grad, up_updated, down_updated


def solution(mesh):
    return jax.shard_map(
        functools.partial(body, mesh.shape["fs"], mesh.shape["tp"]),
        mesh=mesh,
        in_specs=(
            P(("fs", "tp"), None),
            P(("fs", "tp"), None),
            P(("fs", "tp"), None),
            P("fs", "tp"),
            P("fs", "tp"),
            P("fs", "tp"),
            P("fs", "tp"),
        ),
        out_specs=(P(("fs", "tp"), None), P(("fs", "tp"), None), P("fs", "tp"), P("fs", "tp")),
        check_vma=False,
    )
```

profile of v0, /device:TPU:0, one launch (start us, length us, event | category | flops | bytes accessed | tf_op | source)
XLA Modules:
  0.0 180.5 jit_solution(12887519513331900022)
XLA Ops:
  0.6 174.2 %feed_forward_step.1 = (bf16[128,2048]{1,0:T(8,128)(2,1)}, bf16[128,2048]{1,0:T(8,128)(2,1)}, bf16[256,1024]{1,0:T(8,128)(2,1)}, bf16[256,1024]{1,0:T(8,128)(2,1)}) custom-call(bf16[128,2048]{1,0:T(8,128)(2,1)} %later_ref.1, bf16[128,2048]{1,0:T(8,128)(2,1)} %earlier_ref.1, bf16[128,2048]{1,0:T(8,128)(2,1)} %cot_ref.1, bf16[256,1024]{1,0:T(8,128)(2,1)} %up_ref.1, ...), custom_call_target="tpu_custom_call" | custom-call | tf_op jit(solution)/shard_map/feed_forward_step/pallas_call | solution.py:363
  174.8 0.0 copy-start.1
  174.8 3.7 %multiply_add_fusion = (f32[256,1024]{1,0:T(8,128)}, f32[256,1024]{1,0:T(8,128)}) fusion(f32[256,1024]{1,0:T(8,128)} %param.13, bf16[256,1024]{1,0:T(8,128)(2,1)} %get-tuple-element.11, f32[256,1024]{1,0:T(8,128)} %param.12, bf16[256,1024]{1,0:T(8,128)(2,1)} %get-tuple-element.10), kind=kLoop, calls=%fused_computation | loop fusion | flops 1572864 | bytes 5242880 | tf_op jit(solution)/shard_map/add | solution.py:393
  178.5 0.0 copy-done.1
  178.5 0.0 copy-start
  178.5 0.8 copy.13
  179.3 0.4 copy-done
  179.7 0.8 copy.14
Async XLA Ops:
  174.8 3.7 %copy-start.1 = (bf16[128,2048]{1,0:T(8,128)(2,1)S(1)}, bf16[128,2048]{1,0:T(8,128)(2,1)}, u32[]{:S(2)}) copy-start(bf16[128,2048]{1,0:T(8,128)(2,1)} %get-tuple-element.18) | copy-start | bytes 1572868
  178.5 1.2 copy-start
where the time goes:
time: 181 us
  Pallas kernels  174 us (96%)
  other arithmetic  3.68 us (2%)
  local copies, waits for them, and re-layouts  2.03 us (1%)
    pallas_call x1, Pallas kernels, body(): pl.pallas_call(functools.partial(kernel, n, m, parts), out_shape=(jax.Sha...  174 us
    add x1, other arithmetic, body(): down_updated = down_total + down_term.astype(F32) * factor  3.68 us

commit v1 on v0

--- a/solution.py
+++ b/solution.py
@@ -351,16 +351,500 @@
             oy_copy(a, s).wait_send()
 
 
-def body(n, m, later_rows, earlier_rows, cotangent, up_weight, down_weight, up_total, down_total):
-    rows_dev, depth = later_rows.shape
-    blk, width = up_weight.shape
+def plane_kernel(n, chunks,
+                 later_ref, earlier_ref, cot_ref, up_ref, down_ref,
+                 later_out, earlier_out, up_out, down_out,
+                 tok, wts, hid, grads, gl, gr, fin, xbuf, part, dbuf, qa, qb,
+                 t_s, t_r, wx_s, wz_s, w_r, g_s, g_r, f_s, f_r, d_s, d_r, q_s, q_r):
+    rows_dev, depth = later_ref.shape
+    blk, width = up_ref.shape
+    z_size, zrows = n // 2, 2 * blk
+    wide, cw = width // 2, width // 2 // chunks
+    chip_rows = 2 * rows_dev
+    fs, tp = lax.axis_index("fs"), lax.axis_index("tp")
+    z, x, y, c = fs // 2, fs % 2, tp // 2, tp % 2
+    last = z_size - 1
+
+    right = {"fs": ((z + 1) % z_size) * 2 + x, "tp": tp}
+    left = {"fs": ((z + last) % z_size) * 2 + x, "tp": tp}
+    x_next = {"fs": z * 2 + 1 - x, "tp": tp}
+    y_next = {"fs": fs, "tp": (1 - y) * 2 + c}
+    mate = {"fs": fs, "tp": y * 2 + 1 - c}
+
+    barrier = pltpu.get_barrier_semaphore()
+    for other in (right, left, x_next, y_next, mate):
+        pl.semaphore_signal(barrier, inc=1, device_id=other, device_id_type=MESH)
+    pl.semaphore_wait(barrier, 5)
+
+    def remote(src, dst, send, recv, to):
+        return pltpu.make_async_remote_copy(
+            src_ref=src, dst_ref=dst, send_sem=send, recv_sem=recv, device_id=to, device_id_type=MESH)
+
+    def rows_at(start, count):
+        return pl.ds(pl.multiple_of(start, math.gcd(count, 128)), count)
+
+    own_w, own_t = (up_ref, down_ref), (earlier_ref, cot_ref, later_ref)
+
+    def piece(m, h, f):
+        return wts.at[m, h, rows_at(f * blk, blk), :]
+
+    def own_cols(m, h, xx):
+        return own_w[m].at[:, pl.ds(pl.multiple_of(xx * wide + h * cw, cw), cw)]
+
+    def wx_copy(m, h):
+        return remote(own_cols(m, h, 1 - x), piece(m, h, fs), wx_s.at[m, h], w_r.at[m, h, fs], x_next)
+
+    def wz_copy(m, h, f, way, own=False):
+        src = own_cols(m, h, x) if own else piece(m, h, f)
+        return remote(src, piece(m, h, f), wz_s.at[way, m, h, f], w_r.at[m, h, f], left if way else right)
+
+    def w_got(m, h, f):
+        wz_copy(m, h, f, 0).wait_recv()
+
+    def spread(m, h, f, own=False):
+        @pl.when(z < last)
+        def _():
+            wz_copy(m, h, f, 0, own).start()
+
+        @pl.when(z > 0)
+        def _():
+            wz_copy(m, h, f, 1, own).start()
+
+    def from_x(h):
+        for m in range(2):
+            w_got(m, h, z * 2 + 1 - x)
+            spread(m, h, z * 2 + 1 - x)
+
+    def gather_step(h, d):
+        for p in (x, 1 - x):
+            for m in range(2):
+                @pl.when(z >= d)
+                def _():
+                    f = (z - d) * 2 + p
+                    w_got(m, h, f)
+
+                    @pl.when(z < last)
+                    def _():
+                        wz_copy(m, h, f, 0).start()
+
+                @pl.when(z + d < z_size)
+                def _():
+                    f = (z + d) * 2 + p
+                    w_got(m, h, f)
+
+                    @pl.when(z > 0)
+                    def _():
+                        wz_copy(m, h, f, 1).start()
+
+    cut_t = rows_dev * 5 // 8 // 16 * 16
+    moves = (
+        (x, y, 0, rows_dev, x_next),
+        (x, y, 0, rows_dev, y_next),
+        (1 - x, y, 0, cut_t, y_next),
+        (x, 1 - y, cut_t, rows_dev - cut_t, x_next),
+        (x, y, 0, rows_dev, mate),
+        (1 - x, y, 0, rows_dev, mate),
+        (x, 1 - y, 0, rows_dev, mate),
+        (1 - x, 1 - y, 0, cut_t, mate),
+        (1 - x, 1 - y, cut_t, rows_dev - cut_t, mate),
+    )
+
+    def block_at(xx, yy, cc):
+        return ((xx * 2 + yy) * 2 + cc) * rows_dev
+
+    def t_copy(a, k, own=False):
+        xx, yy, lo, count, to = moves[k]
+        there = tok.at[a, rows_at(block_at(xx, yy, c) + lo, count), :]
+        return remote(own_t[a] if own else there, there, t_s.at[a, k], t_r.at[a, k], to)
+
+    def t_first(a):
+        for k in (0, 1, 4):
+            t_copy(a, k, True).start()
+
+    def t_pass(a):
+        t_copy(a, 1).wait_recv()
+        t_copy(a, 3).start()
+        t_copy(a, 6).start()
+        t_copy(a, 0).wait_recv()
+        t_copy(a, 2).start()
+        t_copy(a, 5).start()
+
+    def t_diagonal(a):
+        t_copy(a, 2).wait_recv()
+        t_copy(a, 7).start()
+        t_copy(a, 3).wait_recv()
+        t_copy(a, 8).start()
+
+    def t_wait(a, kinds):
+        for k in kinds:
+            t_copy(a, k).wait_recv()
+
+    def put(dst, dst_row, src, columns, count):
+        step = math.gcd(count, 64)
+
+        @pl.loop(0, count // step)
+        def _(i):
+            o = pl.multiple_of(i * step, step)
+            dst[pl.ds(pl.multiple_of(dst_row + o, step), step), :] = src[pl.ds(o, step), columns]
+
+    def chip_at(i):
+        return (((x + i % 2) % 2) * 2 + (y + i // 2) % 2) * chip_rows
+
+    def earlier_hidden(h, lo, hi):
+        @pl.loop(lo, hi)
+        def _(i):
+            o = rows_at(chip_at(i), chip_rows)
+            relu = jnp.maximum(jnp.dot(tok[0, o, :], wts[0, h], preferred_element_type=F32), 0.0)
+            got = jnp.dot(tok[1, o, :], wts[1, h], preferred_element_type=F32)
+            hid[0, h, o, :] = (2.0 * relu * got).astype(BF16)
+            hid[1, h, o, :] = (relu * relu).astype(BF16)
+
+    def later_hidden(h):
+        @pl.loop(0, 4)
+        def _(i):
+            o = rows_at(i * chip_rows, chip_rows)
+            relu = jnp.maximum(jnp.dot(tok[2, o, :], wts[0, h], preferred_element_type=F32), 0.0)
+            hid[2, h, o, :] = (relu * relu).astype(BF16)
+
+    def term(m, h, d):
+        o = rows_at(d * zrows, zrows)
+        grads[m, h, o, :] = lax.dot_general(
+            tok[m, :, o], hid[m, h], (((0,), (0,)), ((), ())), preferred_element_type=F32).astype(BF16)
+
+    def g_copy(m, h, d, way):
+        src = grads.at[m, h, rows_at(d * zrows, zrows), :]
+        return remote(src, (gr if way else gl).at[m, h, d], g_s.at[way, m, h, d], g_r.at[way, m, h, d],
+                      left if way else right)
+
+    def terms(h):
+        @pl.loop(0, last)
+        def _(k):
+            @pl.when(last - k > z)
+            def _():
+                @pl.loop(0, 2)
+                def _(m):
+                    term(m, h, last - k)
+
+                    @pl.when(z == 0)
+                    def _():
+                        g_copy(m, h, last - k, 0).start()
+
+            @pl.when(k < z)
+            def _():
+                @pl.loop(0, 2)
+                def _(m):
+                    term(m, h, k)
+
+                    @pl.when(z == last)
+                    def _():
+                        g_copy(m, h, k, 1).start()
+
+        @pl.loop(0, 2)
+        def _(m):
+            term(m, h, z)
+
+    def add_rows(dst, dst_row, src, count):
+        step = math.gcd(count, 32)
+
+        @pl.loop(0, count // step)
+        def _(i):
+            o = pl.multiple_of(i * step, step)
+            at = pl.ds(pl.multiple_of(dst_row + o, math.gcd(step, 16)), step)
+            dst[at, :] = (dst[at, :].astype(F32) + src[pl.ds(o, step), :].astype(F32)).astype(BF16)
+
+    def reduce_step(h, k):
+        for m in range(2):
+            @pl.when((last - k > z) & (z > 0))
+            def _():
+                d = last - k
+                g_copy(m, h, d, 0).wait_recv()
+                add_rows(grads.at[m, h], d * zrows, gl.at[m, h, d], zrows)
+                g_copy(m, h, d, 0).start()
+
+            @pl.when((k < z) & (z < last))
+            def _():
+                g_copy(m, h, k, 1).wait_recv()
+                add_rows(grads.at[m, h], k * zrows, gr.at[m, h, k], zrows)
+                g_copy(m, h, k, 1).start()
+
+    outs = (up_out, down_out)
+
+    def f_copy(m, h):
+        return remote(fin.at[m, h], xbuf.at[m, h], f_s.at[m, h], f_r.at[m, h], x_next)
+
+    def total(m, h, xx, dst, columns, sources):
+        step = math.gcd(blk, 32)
+
+        @pl.loop(0, blk // step)
+        def _(i):
+            o = pl.multiple_of(i * step, step)
+            at = pl.ds(pl.multiple_of(xx * blk + o, step), step)
+            got = grads[m, h, pl.ds(pl.multiple_of(z * zrows + xx * blk + o, step), step), :].astype(F32)
+            for src in sources:
+                got += src[m, h, z, at, :].astype(F32)
+            dst[pl.ds(o, step), columns] = got.astype(BF16)
+
+    def finish(h):
+        mine = pl.ds(pl.multiple_of(x * wide + h * cw, cw), cw)
+        for m in range(2):
+            @pl.when(z > 0)
+            def _():
+                g_copy(m, h, z, 0).wait_recv()
+
+            @pl.when(z < last)
+            def _():
+                g_copy(m, h, z, 1).wait_recv()
+
+            for case, sources in ((z == 0, (gr,)), (z == last, (gl,)), ((z > 0) & (z < last), (gl, gr))):
+                @pl.when(case)
+                def _():
+                    total(m, h, 1 - x, fin.at[m, h], slice(None), sources)
+
+            f_copy(m, h).start()
+            for case, sources in ((z == 0, (gr,)), (z == last, (gl,)), ((z > 0) & (z < last), (gl, gr))):
+                @pl.when(case)
+                def _():
+                    total(m, h, x, outs[m], mine, sources)
+
+    def finish_x(h):
+        theirs = pl.ds(pl.multiple_of((1 - x) * wide + h * cw, cw), cw)
+        step = math.gcd(blk, 32)
+        for m in range(2):
+            f_copy(m, h).wait_recv()
+
+            @pl.loop(0, blk // step)
+            def _(i):
+                o = pl.ds(pl.multiple_of(i * step, step), step)
+                outs[m][o, theirs] = xbuf[m, h, o, :]
+
+    tile = math.gcd(depth, 256)
+
+    def partial(a, k, w):
+        @pl.loop(0, depth // tile)
+        def _(j):
+            o = pl.ds(pl.multiple_of(j * tile, tile), tile)
+            got = None
+            for h in range(chunks):
+                one = lax.dot_general(hid[k, h], wts[w, h, o, :], (((1,), (1,)), ((), ())),
+                                      preferred_element_type=F32)
+                got = one if got is None else got + one
+            part[a, :, o] = got.astype(BF16)
+
+    def d_copy(a, q):
+        return remote(part.at[a, rows_at(q * chip_rows + (1 - c) * rows_dev, rows_dev), :], dbuf.at[a, q],
+                      d_s.at[a, q], d_r.at[a, q], mate)
+
+    def d_start(a):
+        for q in range(4):
+            d_copy(a, q).start()
+
+    cut_q = rows_dev * 3 // 8 // 16 * 16
+    low, high = (0, cut_q), (cut_q, rows_dev - cut_q)
+    hops = (
+        (1 - x, y, low, qa, 0, x_next),
+        (1 - x, 1 - y, low, qa, 1, x_next),
+        (x, 1 - y, high, qb, 0, y_next),
+        (1 - x, 1 - y, high, qb, 1, y_next),
+        (x, 1 - y, low, qa, 2, y_next),
+        (1 - x, y, high, qb, 2, x_next),
+    )
+
+    def q_copy(a, k):
+        xx, yy, (lo, count), buf, slot, to = hops[k]
+        return remote(part.at[a, rows_at(block_at(xx, yy, c) + lo, count), :], buf.at[a, slot],
+                      q_s.at[a, k], q_r.at[a, k], to)
+
+    def q_first(a):
+        for q in range(4):
+            d_copy(a, q).wait_recv()
+            add_rows(part.at[a], q * chip_rows + c * rows_dev, dbuf.at[a, q], rows_dev)
+        for k in range(4):
+            q_copy(a, k).start()
+
+    def q_second(a):
+        q_copy(a, 1).wait_recv()
+        add_rows(part.at[a], block_at(x, 1 - y, c), qa.at[a, 1], cut_q)
+        q_copy(a, 4).start()
+        q_copy(a, 3).wait_recv()
+        add_rows(part.at[a], block_at(1 - x, y, c) + cut_q, qb.at[a, 1], rows_dev - cut_q)
+        q_copy(a, 5).start()
+
+    def q_last(a, out):
+        for k in (0, 4, 2, 5):
+            q_copy(a, k).wait_recv()
+        for (lo, count), buf in ((low, qa), (high, qb)):
+            step = math.gcd(count, 16)
+
+            @pl.loop(0, count // step)
+            def _(i):
+                o = pl.multiple_of(i * step, step)
+                at = pl.ds(o, step)
+                own = pl.ds(pl.multiple_of(block_at(x, y, c) + lo + o, step), step)
+                out[pl.ds(pl.multiple_of(lo + o, step), step), :] = (
+                    part[a, own, :].astype(F32) + buf[a, 0, at, :].astype(F32) + buf[a, 2, at, :].astype(F32)
+                ).astype(BF16)
+
+    for m in range(2):
+        wx_copy(m, 0).start()
+    for m in range(2):
+        spread(m, 0, fs, True)
+    t_first(0)
+    t_first(1)
+    for m in range(2):
+        for h in range(chunks):
+            cols = pl.ds(pl.multiple_of(x * wide + h * cw, cw), cw)
+            put(wts.at[m, h], fs * blk, own_w[m], cols, blk)
+    for a in range(3):
+        put(tok.at[a], block_at(x, y, c), own_t[a], slice(None), rows_dev)
+    from_x(0)
+    gather_step(0, 1)
+    t_pass(0)
+    for d in range(2, last):
+        gather_step(0, d)
+    t_pass(1)
+    for h in range(1, chunks):
+        for m in range(2):
+            wx_copy(m, h).start()
+            spread(m, h, fs, True)
+    t_first(2)
+    gather_step(0, last)
+    for a in range(2):
+        t_wait(a, (4, 5, 6))
+    earlier_hidden(0, 0, 3)
+    for a in range(2):
+        t_diagonal(a)
+    for a in range(2):
+        t_wait(a, (7, 8))
+    earlier_hidden(0, 3, 4)
+    terms(0)
+    for h in range(1, chunks):
+        from_x(h)
+        gather_step(h, 1)
+    reduce_step(0, 0)
+    t_pass(2)
+    for h in range(1, chunks):
+        for d in range(2, last):
+            gather_step(h, d)
+    for k in range(1, last - 1):
+        reduce_step(0, k)
+    t_diagonal(2)
+    t_wait(2, (4, 5, 6, 7, 8))
+    later_hidden(0)
+    for h in range(1, chunks):
+        gather_step(h, last)
+        earlier_hidden(h, 0, 4)
+        terms(h)
+    partial(0, 0, 0)
+    d_start(0)
+    for h in range(1, chunks):
+        later_hidden(h)
+    reduce_step(0, last - 1)
+    finish(0)
+    partial(1, 2, 1)
+    d_start(1)
+    q_first(0)
+    q_first(1)
+    for h in range(1, chunks):
+        reduce_step(h, 0)
+    q_second(0)
+    for h in range(1, chunks):
+        for k in range(1, last - 1):
+            reduce_step(h, k)
+    finish_x(0)
+    q_second(1)
+    q_last(0, earlier_out)
+    for h in range(1, chunks):
+        reduce_step(h, last - 1)
+        finish(h)
+    q_last(1, later_out)
+    for h in range(1, chunks):
+        finish_x(h)
+
+    for m in range(2):
+        for h in range(chunks):
+            wx_copy(m, h).wait_send()
+            f_copy(m, h).wait_send()
+
+            @pl.loop(0, n)
+            def _(f):
+                @pl.when((f // 2 <= z) & (z < last))
+                def _():
+                    wz_copy(m, h, f, 0).wait_send()
+
+                @pl.when((f // 2 >= z) & (z > 0))
+                def _():
+                    wz_copy(m, h, f, 1).wait_send()
+
+            @pl.loop(0, z_size)
+            def _(d):
+                @pl.when(d > z)
+                def _():
+                    g_copy(m, h, d, 0).wait_send()
+
+                @pl.when(d < z)
+                def _():
+                    g_copy(m, h, d, 1).wait_send()
+    for a in range(3):
+        for k in range(9):
+            t_copy(a, k).wait_send()
+    for a in range(2):
+        for q in range(4):
+            d_copy(a, q).wait_send()
+        for k in range(6):
+            q_copy(a, k).wait_send()
+
+
+def plane_call(n, m, *args):
+    rows_dev, depth = args[0].shape
+    blk, width = args[3].shape
+    z_size, chunks, rows = n // 2, 2, rows_dev * 8
+    cw = width // 2 // chunks
+    cut_q = rows_dev * 3 // 8 // 16 * 16
+    dma = pltpu.SemaphoreType.DMA
+    vmem = pl.BlockSpec(memory_space=pltpu.VMEM)
+    return pl.pallas_call(
+        functools.partial(plane_kernel, n, chunks),
+        out_shape=(
+            jax.ShapeDtypeStruct((rows_dev, depth), BF16),
+            jax.ShapeDtypeStruct((rows_dev, depth), BF16),
+            jax.ShapeDtypeStruct((blk, width), BF16),
+            jax.ShapeDtypeStruct((blk, width), BF16),
+        ),
+        in_specs=[vmem] * 5,
+        out_specs=(vmem,) * 4,
+        scratch_shapes=[
+            pltpu.VMEM((3, rows, depth), BF16),
+            pltpu.VMEM((2, chunks, depth, cw), BF16),
+            pltpu.VMEM((3, chunks, rows, cw), BF16),
+            pltpu.VMEM((2, chunks, depth, cw), BF16),
+            pltpu.VMEM((2, chunks, z_size, 2 * blk, cw), BF16),
+            pltpu.VMEM((2, chunks, z_size, 2 * blk, cw), BF16),
+            pltpu.VMEM((2, chunks, blk, cw), BF16),
+            pltpu.VMEM((2, chunks, blk, cw), BF16),
+            pltpu.VMEM((2, rows, depth), BF16),
+            pltpu.VMEM((2, 4, rows_dev, depth), BF16),
+            pltpu.VMEM((2, 3, cut_q, depth), BF16),
+            pltpu.VMEM((2, 3, rows_dev - cut_q, depth), BF16),
+            dma((3, 9)), dma((3, 9)), dma((2, chunks)), dma((2, 2, chunks, n)), dma((2, chunks, n)),
+            dma((2, 2, chunks, z_size)), dma((2, 2, chunks, z_size)), dma((2, chunks)), dma((2, chunks)),
+            dma((2, 4)), dma((2, 4)), dma((2, 6)), dma((2, 6)),
+        ],
+        compiler_params=pltpu.CompilerParams(
+            collective_id=0, has_side_effects=True, vmem_limit_bytes=67043328
+        ),
+        name="feed_forward_planes",
+    )(*args)
+
+
+def ring_call(n, m, *args):
+    rows_dev, depth = args[0].shape
+    blk, width = args[3].shape
     rows, half, y_size = rows_dev * m, n // 2, m // 2
-    factor = 1.0 / math.sqrt(rows * n)
     dma = pltpu.SemaphoreType.DMA
     vmem = pl.BlockSpec(memory_space=pltpu.VMEM)
     sums = max(y_size - 1, 1)
     parts = 2 if width % 256 == 0 else 1
-    later_out, earlier_grad, up_term, down_term = pl.pallas_call(
+    return pl.pallas_call(
         functools.partial(kernel, n, m, parts),
         out_shape=(
             jax.ShapeDtypeStruct((rows_dev, depth), BF16),
@@ -388,7 +872,16 @@
             collective_id=0, has_side_effects=True, vmem_limit_bytes=67043328
         ),
         name="feed_forward_step",
-    )(later_rows, earlier_rows, cotangent, up_weight, down_weight)
+    )(*args)
+
+
+def body(n, m, later_rows, earlier_rows, cotangent, up_weight, down_weight, up_total, down_total):
+    rows = later_rows.shape[0] * m
+    factor = 1.0 / math.sqrt(rows * n)
+    width = up_weight.shape[1]
+    planar = columns_of(n) == 2 and n > 4 and m == 4 and width % 1024 == 0 and rows % 512 == 0
+    later_out, earlier_grad, up_term, down_term = (plane_call if planar else ring_call)(
+        n, m, later_rows, earlier_rows, cotangent, up_weight, down_weight)
     up_updated = up_total + up_term.astype(F32) * factor
     down_updated = down_total + down_term.astype(F32) * factor
     return later_out, earlier_grad, up_updated, down_updated

time: 181 us -> 208 us (1.15)
  Pallas kernels: 174 us -> 202 us
    pallas_call x1, Pallas kernels: 174 us -> 202 us  [plane_call(): pl.pallas_call(functools.partial(plane_kernel, n, chunks), out_shape=(jax...]
where the time goes in v1:
time: 208 us
  Pallas kernels  202 us (97%)
  other arithmetic  3.68 us (2%)
    pallas_call x1, Pallas kernels, plane_call(): pl.pallas_call(functools.partial(plane_kernel, n, chunks), out_shape=(jax...  202 us

profile of v1, /device:TPU:0, one launch (start us, length us, event | category | flops | bytes accessed | tf_op | source)
XLA Modules:
  0.0 208.0 jit_solution(17425880305303612167)
XLA Ops:
  0.6 201.6 %feed_forward_planes.1 = (bf16[128,2048]{1,0:T(8,128)(2,1)}, bf16[128,2048]{1,0:T(8,128)(2,1)}, bf16[256,1024]{1,0:T(8,128)(2,1)}, bf16[256,1024]{1,0:T(8,128)(2,1)}) custom-call(bf16[128,2048]{1,0:T(8,128)(2,1)} %later_ref.1, bf16[128,2048]{1,0:T(8,128)(2,1)} %earlier_ref.1, bf16[128,2048]{1,0:T(8,128)(2,1)} %cot_ref.1, bf16[256,1024]{1,0:T(8,128)(2,1)} %up_ref.1, ...), custom_call_target="tpu_custom_call" | custom-call | tf_op jit(solution)/shard_map/feed_forward_planes/pallas_call | solution.py:805
  202.3 0.0 copy-start.1
  202.3 3.7 %multiply_add_fusion = (f32[256,1024]{1,0:T(8,128)}, f32[256,1024]{1,0:T(8,128)}) fusion(f32[256,1024]{1,0:T(8,128)} %param.13, bf16[256,1024]{1,0:T(8,128)(2,1)} %get-tuple-element.11, f32[256,1024]{1,0:T(8,128)} %param.12, bf16[256,1024]{1,0:T(8,128)(2,1)} %get-tuple-element.10), kind=kLoop, calls=%fused_computation | loop fusion | flops 1572864 | bytes 5242880 | tf_op jit(solution)/shard_map/add | solution.py:886
  206.0 0.0 copy-done.1
  206.0 0.0 copy-start
  206.0 0.8 copy.13
  206.8 0.4 copy-done
  207.2 0.8 copy.14
Async XLA Ops:
  202.3 3.7 %copy-start.1 = (bf16[128,2048]{1,0:T(8,128)(2,1)S(1)}, bf16[128,2048]{1,0:T(8,128)(2,1)}, u32[]{:S(2)}) copy-start(bf16[128,2048]{1,0:T(8,128)(2,1)} %get-tuple-element.18) | copy-start | bytes 1572868
  206.0 1.2 copy-start

commit v2 on v1

--- a/solution.py
+++ b/solution.py
@@ -354,7 +354,7 @@
 def plane_kernel(n, chunks,
                  later_ref, earlier_ref, cot_ref, up_ref, down_ref,
                  later_out, earlier_out, up_out, down_out,
-                 tok, wts, hid, grads, gl, gr, fin, xbuf, part, dbuf, qa, qb,
+                 tok, wts, hid, grads, gbuf, fin, xbuf, part, dbuf, qa, qb,
                  t_s, t_r, wx_s, wz_s, w_r, g_s, g_r, f_s, f_r, d_s, d_r, q_s, q_r):
     rows_dev, depth = later_ref.shape
     blk, width = up_ref.shape
@@ -410,33 +410,35 @@
         def _():
             wz_copy(m, h, f, 1, own).start()
 
-    def from_x(h):
-        for m in range(2):
+    def from_x(h, ms=(0, 1)):
+        for m in ms:
             w_got(m, h, z * 2 + 1 - x)
             spread(m, h, z * 2 + 1 - x)
 
-    def gather_step(h, d):
-        for p in (x, 1 - x):
-            for m in range(2):
-                @pl.when(z >= d)
+    def relay(h, d, columns=(0, 1), ms=(0, 1)):
+        for m in ms:
+            for p in columns:
+                p = (x + p) % 2
+
+                @pl.when((z >= d) & (z < last))
                 def _():
-                    f = (z - d) * 2 + p
-                    w_got(m, h, f)
-
-                    @pl.when(z < last)
-                    def _():
-                        wz_copy(m, h, f, 0).start()
-
-                @pl.when(z + d < z_size)
+                    w_got(m, h, (z - d) * 2 + p)
+                    wz_copy(m, h, (z - d) * 2 + p, 0).start()
+
+                @pl.when((z + d < z_size) & (z > 0))
                 def _():
-                    f = (z + d) * 2 + p
-                    w_got(m, h, f)
-
-                    @pl.when(z > 0)
-                    def _():
-                        wz_copy(m, h, f, 1).start()
-
-    cut_t = rows_dev * 5 // 8 // 16 * 16
+                    w_got(m, h, (z + d) * 2 + p)
+                    wz_copy(m, h, (z + d) * 2 + p, 1).start()
+
+    def settle(h, m):
+        @pl.when((z == 0) | (z == last))
+        def _():
+            @pl.loop(1, z_size)
+            def _(d):
+                for p in range(2):
+                    w_got(m, h, (z + d) % z_size * 2 + p)
+
+    cut_t = rows_dev * 3 // 4 // 16 * 16
     moves = (
         (x, y, 0, rows_dev, x_next),
         (x, y, 0, rows_dev, y_next),
@@ -461,10 +463,12 @@
         for k in (0, 1, 4):
             t_copy(a, k, True).start()
 
-    def t_pass(a):
+    def t_pass_y(a):
         t_copy(a, 1).wait_recv()
         t_copy(a, 3).start()
         t_copy(a, 6).start()
+
+    def t_pass_x(a):
         t_copy(a, 0).wait_recv()
         t_copy(a, 2).start()
         t_copy(a, 5).start()
@@ -513,11 +517,11 @@
 
     def g_copy(m, h, d, way):
         src = grads.at[m, h, rows_at(d * zrows, zrows), :]
-        return remote(src, (gr if way else gl).at[m, h, d], g_s.at[way, m, h, d], g_r.at[way, m, h, d],
-                      left if way else right)
-
-    def terms(h):
-        @pl.loop(0, last)
+        to = {"fs": ((z + z_size + 1 - 2 * way) % z_size) * 2 + x, "tp": tp}
+        return remote(src, gbuf.at[way, m, h, d], g_s.at[way, m, h, d], g_r.at[way, m, h, d], to)
+
+    def terms(h, lo, hi):
+        @pl.loop(lo, hi)
         def _(k):
             @pl.when(last - k > z)
             def _():
@@ -539,6 +543,7 @@
                     def _():
                         g_copy(m, h, k, 1).start()
 
+    def own_terms(h):
         @pl.loop(0, 2)
         def _(m):
             term(m, h, z)
@@ -552,20 +557,19 @@
             at = pl.ds(pl.multiple_of(dst_row + o, math.gcd(step, 16)), step)
             dst[at, :] = (dst[at, :].astype(F32) + src[pl.ds(o, step), :].astype(F32)).astype(BF16)
 
-    def reduce_step(h, k):
-        for m in range(2):
-            @pl.when((last - k > z) & (z > 0))
-            def _():
-                d = last - k
-                g_copy(m, h, d, 0).wait_recv()
-                add_rows(grads.at[m, h], d * zrows, gl.at[m, h, d], zrows)
-                g_copy(m, h, d, 0).start()
-
-            @pl.when((k < z) & (z < last))
-            def _():
-                g_copy(m, h, k, 1).wait_recv()
-                add_rows(grads.at[m, h], k * zrows, gr.at[m, h, k], zrows)
-                g_copy(m, h, k, 1).start()
+    side = 2 * z // z_size
+
+    def reduce_step(h, k, m, near):
+        way = side if near else 1 - side
+        d = (1 - way) * (last - k) + way * k
+        beyond = (1 - 2 * way) * (d - z)
+        behind = (1 - way) * z + way * (last - z)
+
+        @pl.when((beyond > 0) & (behind > 0))
+        def _():
+            g_copy(m, h, d, way).wait_recv()
+            add_rows(grads.at[m, h], d * zrows, gbuf.at[way, m, h, d], zrows)
+            g_copy(m, h, d, way).start()
 
     outs = (up_out, down_out)
 
@@ -581,12 +585,12 @@
             at = pl.ds(pl.multiple_of(xx * blk + o, step), step)
             got = grads[m, h, pl.ds(pl.multiple_of(z * zrows + xx * blk + o, step), step), :].astype(F32)
             for src in sources:
-                got += src[m, h, z, at, :].astype(F32)
+                got += gbuf[src, m, h, z, at, :].astype(F32)
             dst[pl.ds(o, step), columns] = got.astype(BF16)
 
-    def finish(h):
+    def finish(h, ms=(0, 1)):
         mine = pl.ds(pl.multiple_of(x * wide + h * cw, cw), cw)
-        for m in range(2):
+        for m in ms:
             @pl.when(z > 0)
             def _():
                 g_copy(m, h, z, 0).wait_recv()
@@ -595,13 +599,13 @@
             def _():
                 g_copy(m, h, z, 1).wait_recv()
 
-            for case, sources in ((z == 0, (gr,)), (z == last, (gl,)), ((z > 0) & (z < last), (gl, gr))):
+            for case, sources in ((z == 0, (1,)), (z == last, (0,)), ((z > 0) & (z < last), (0, 1))):
                 @pl.when(case)
                 def _():
                     total(m, h, 1 - x, fin.at[m, h], slice(None), sources)
 
             f_copy(m, h).start()
-            for case, sources in ((z == 0, (gr,)), (z == last, (gl,)), ((z > 0) & (z < last), (gl, gr))):
+            for case, sources in ((z == 0, (1,)), (z == last, (0,)), ((z > 0) & (z < last), (0, 1))):
                 @pl.when(case)
                 def _():
                     total(m, h, x, outs[m], mine, sources)
@@ -691,74 +695,83 @@
     t_first(0)
     t_first(1)
     for m in range(2):
+        wx_copy(m, 1).start()
+    for m in range(2):
         for h in range(chunks):
             cols = pl.ds(pl.multiple_of(x * wide + h * cw, cw), cw)
             put(wts.at[m, h], fs * blk, own_w[m], cols, blk)
     for a in range(3):
         put(tok.at[a], block_at(x, y, c), own_t[a], slice(None), rows_dev)
     from_x(0)
-    gather_step(0, 1)
-    t_pass(0)
-    for d in range(2, last):
-        gather_step(0, d)
-    t_pass(1)
-    for h in range(1, chunks):
-        for m in range(2):
-            wx_copy(m, h).start()
-            spread(m, h, fs, True)
+    relay(0, 1)
+    t_pass_y(0)
+    t_pass_x(0)
+    relay(0, 2)
+    t_pass_y(1)
+    t_pass_x(1)
+    for m in range(2):
+        spread(m, 1, fs, True)
     t_first(2)
-    gather_step(0, last)
+    settle(0, 0)
+    settle(0, 1)
     for a in range(2):
         t_wait(a, (4, 5, 6))
     earlier_hidden(0, 0, 3)
-    for a in range(2):
-        t_diagonal(a)
+    from_x(1)
+    t_diagonal(0)
+    relay(1, 1, (0,))
+    t_diagonal(1)
     for a in range(2):
         t_wait(a, (7, 8))
     earlier_hidden(0, 3, 4)
-    terms(0)
-    for h in range(1, chunks):
-        from_x(h)
-        gather_step(h, 1)
-    reduce_step(0, 0)
-    t_pass(2)
-    for h in range(1, chunks):
-        for d in range(2, last):
-            gather_step(h, d)
-    for k in range(1, last - 1):
-        reduce_step(0, k)
+    terms(0, 0, last)
+    own_terms(0)
+    t_pass_y(2)
+    relay(1, 1, (1,), (0,))
+    relay(1, 2, (0,), (0,))
+    reduce_step(0, 0, 0, True)
+    t_pass_x(2)
+    relay(1, 2, (1,), (0,))
+    relay(1, 1, (1,), (1,))
+    relay(1, 2, (0,), (1,))
+    reduce_step(0, 0, 1, True)
+    relay(1, 2, (1,), (1,))
+    reduce_step(0, 0, 0, False)
     t_diagonal(2)
+    settle(1, 0)
     t_wait(2, (4, 5, 6, 7, 8))
     later_hidden(0)
-    for h in range(1, chunks):
-        gather_step(h, last)
-        earlier_hidden(h, 0, 4)
-        terms(h)
+    later_hidden(1)
+    reduce_step(0, 1, 0, True)
+    reduce_step(0, 0, 1, False)
+    settle(1, 1)
+    partial(1, 2, 1)
+    d_start(1)
+    earlier_hidden(1, 0, 4)
+    reduce_step(0, 1, 1, True)
+    terms(1, 0, 1)
+    q_first(1)
+    terms(1, 1, last)
+    own_terms(1)
     partial(0, 0, 0)
     d_start(0)
-    for h in range(1, chunks):
-        later_hidden(h)
-    reduce_step(0, last - 1)
-    finish(0)
-    partial(1, 2, 1)
-    d_start(1)
+    finish(0, (0,))
+    finish(0, (1,))
     q_first(0)
-    q_first(1)
-    for h in range(1, chunks):
-        reduce_step(h, 0)
+    reduce_step(1, 0, 0, True)
+    reduce_step(1, 0, 1, True)
+    q_second(1)
+    reduce_step(1, 0, 0, False)
+    finish_x(0)
+    reduce_step(1, 1, 0, True)
+    reduce_step(1, 0, 1, False)
+    reduce_step(1, 1, 1, True)
     q_second(0)
-    for h in range(1, chunks):
-        for k in range(1, last - 1):
-            reduce_step(h, k)
-    finish_x(0)
-    q_second(1)
+    q_last(1, later_out)
     q_last(0, earlier_out)
-    for h in range(1, chunks):
-        reduce_step(h, last - 1)
-        finish(h)
-    q_last(1, later_out)
-    for h in range(1, chunks):
-        finish_x(h)
+    finish(1, (0,))
+    finish(1, (1,))
+    finish_x(1)
 
     for m in range(2):
         for h in range(chunks):
@@ -817,8 +830,7 @@
             pltpu.VMEM((2, chunks, depth, cw), BF16),
             pltpu.VMEM((3, chunks, rows, cw), BF16),
             pltpu.VMEM((2, chunks, depth, cw), BF16),
-            pltpu.VMEM((2, chunks, z_size, 2 * blk, cw), BF16),
-            pltpu.VMEM((2, chunks, z_size, 2 * blk, cw), BF16),
+            pltpu.VMEM((2, 2, chunks, z_size, 2 * blk, cw), BF16),
             pltpu.VMEM((2, chunks, blk, cw), BF16),
             pltpu.VMEM((2, chunks, blk, cw), BF16),
             pltpu.VMEM((2, rows, depth), BF16),
@@ -879,7 +891,7 @@
     rows = later_rows.shape[0] * m
     factor = 1.0 / math.sqrt(rows * n)
     width = up_weight.shape[1]
-    planar = columns_of(n) == 2 and n > 4 and m == 4 and width % 1024 == 0 and rows % 512 == 0
+    planar = columns_of(n) == 2 and n == 8 and m == 4 and width % 1024 == 0 and rows % 512 == 0
     later_out, earlier_grad, up_term, down_term = (plane_call if planar else ring_call)(
         n, m, later_rows, earlier_rows, cotangent, up_weight, down_weight)
     up_updated = up_total + up_term.astype(F32) * factor

time: 208 us -> 142 us (0.68)
  Pallas kernels: 202 us -> 135 us
    pallas_call x1, Pallas kernels: 202 us -> 135 us  [plane_call(): pl.pallas_call(functools.partial(plane_kernel, n, chunks), out_shape=(jax...]
where the time goes in v2:
time: 142 us; the launch traced here: 141 us
  Pallas kernels  135 us (95%)
  other arithmetic  3.68 us (3%)
  local copies, waits for them, and re-layouts  2.03 us (1%)
    pallas_call x1, Pallas kernels, plane_call(): pl.pallas_call(functools.partial(plane_kernel, n, chunks), out_shape=(jax...  135 us
    add x1, other arithmetic, body(): down_updated = down_total + down_term.astype(F32) * factor  3.68 us

profile of v2, /device:TPU:0, one launch (start us, length us, event | category | flops | bytes accessed | tf_op | source)
XLA Modules:
  0.0 141.3 jit_solution(3492391367680030064)
XLA Ops:
  0.6 135.0 %feed_forward_planes.1 = (bf16[128,2048]{1,0:T(8,128)(2,1)}, bf16[128,2048]{1,0:T(8,128)(2,1)}, bf16[256,1024]{1,0:T(8,128)(2,1)}, bf16[256,1024]{1,0:T(8,128)(2,1)}) custom-call(bf16[128,2048]{1,0:T(8,128)(2,1)} %later_ref.1, bf16[128,2048]{1,0:T(8,128)(2,1)} %earlier_ref.1, bf16[128,2048]{1,0:T(8,128)(2,1)} %cot_ref.1, bf16[256,1024]{1,0:T(8,128)(2,1)} %up_ref.1, ...), custom_call_target="tpu_custom_call" | custom-call | tf_op jit(solution)/shard_map/feed_forward_planes/pallas_call | solution.py:818
  135.6 0.0 copy-start.1
  135.6 3.7 %multiply_add_fusion = (f32[256,1024]{1,0:T(8,128)}, f32[256,1024]{1,0:T(8,128)}) fusion(f32[256,1024]{1,0:T(8,128)} %param.13, bf16[256,1024]{1,0:T(8,128)(2,1)} %get-tuple-element.11, f32[256,1024]{1,0:T(8,128)} %param.12, bf16[256,1024]{1,0:T(8,128)(2,1)} %get-tuple-element.10), kind=kLoop, calls=%fused_computation | loop fusion | flops 1572864 | bytes 5242880 | tf_op jit(solution)/shard_map/add | solution.py:898
  139.3 0.0 copy-done.1
  139.3 0.0 copy-start
  139.3 0.8 copy.13
  140.1 0.4 copy-done
  140.5 0.8 copy.14
Async XLA Ops:
  135.6 3.7 %copy-start.1 = (bf16[128,2048]{1,0:T(8,128)(2,1)S(1)}, bf16[128,2048]{1,0:T(8,128)(2,1)}, u32[]{:S(2)}) copy-start(bf16[128,2048]{1,0:T(8,128)(2,1)} %get-tuple-element.18) | copy-start | bytes 1572868
  139.3 1.2 copy-start

commit v3 on v2

--- a/solution.py
+++ b/solution.py
@@ -351,11 +351,11 @@
             oy_copy(a, s).wait_send()
 
 
-def plane_kernel(n, chunks,
-                 later_ref, earlier_ref, cot_ref, up_ref, down_ref,
+def plane_kernel(n, chunks, factor,
+                 later_ref, earlier_ref, cot_ref, up_ref, down_ref, up_total, down_total,
                  later_out, earlier_out, up_out, down_out,
-                 tok, wts, hid, grads, gbuf, fin, xbuf, part, dbuf, qa, qb,
-                 t_s, t_r, wx_s, wz_s, w_r, g_s, g_r, f_s, f_r, d_s, d_r, q_s, q_r):
+                 tok, wts, hid, grads, gbuf, fin, xbuf, part, dbuf, qa, qb, stage, sums,
+                 l_s, o_s, t_s, t_r, wx_s, wz_s, w_r, g_s, g_r, f_s, f_r, d_s, d_r, q_s, q_r, q_l):
     rows_dev, depth = later_ref.shape
     blk, width = up_ref.shape
     z_size, zrows = n // 2, 2 * blk
@@ -371,6 +371,38 @@
     y_next = {"fs": fs, "tp": (1 - y) * 2 + c}
     mate = {"fs": fs, "tp": y * 2 + 1 - c}
 
+    def block_at(xx, yy, cc):
+        return ((xx * 2 + yy) * 2 + cc) * rows_dev
+
+    def rows_at(start, count):
+        return pl.ds(pl.multiple_of(start, math.gcd(count, 128)), count)
+
+    def columns_at(xx, h):
+        return pl.ds(pl.multiple_of(xx * wide + h * cw, cw), cw)
+
+    own_w, own_t = (up_ref, down_ref), (earlier_ref, cot_ref, later_ref)
+
+    def load_w(m, h):
+        return pltpu.make_async_copy(
+            own_w[m].at[:, columns_at(x, h)], wts.at[m, h, rows_at(fs * blk, blk), :], l_s.at[m * chunks + h])
+
+    def load_t(a):
+        return pltpu.make_async_copy(
+            own_t[a], tok.at[a, rows_at(block_at(x, y, c), rows_dev), :], l_s.at[2 * chunks + a])
+
+    for m in range(2):
+        load_w(m, 0).start()
+    load_t(0).start()
+    load_t(1).start()
+    for m in range(2):
+        load_w(m, 1).start()
+    load_t(2).start()
+    totals = tuple(
+        pltpu.make_async_copy(total, sums.at[m], l_s.at[2 * chunks + 3 + m])
+        for m, total in enumerate((up_total, down_total)))
+    for m in range(2):
+        totals[m].start()
+
     barrier = pltpu.get_barrier_semaphore()
     for other in (right, left, x_next, y_next, mate):
         pl.semaphore_signal(barrier, inc=1, device_id=other, device_id_type=MESH)
@@ -380,35 +412,26 @@
         return pltpu.make_async_remote_copy(
             src_ref=src, dst_ref=dst, send_sem=send, recv_sem=recv, device_id=to, device_id_type=MESH)
 
-    def rows_at(start, count):
-        return pl.ds(pl.multiple_of(start, math.gcd(count, 128)), count)
-
-    own_w, own_t = (up_ref, down_ref), (earlier_ref, cot_ref, later_ref)
-
     def piece(m, h, f):
         return wts.at[m, h, rows_at(f * blk, blk), :]
 
-    def own_cols(m, h, xx):
-        return own_w[m].at[:, pl.ds(pl.multiple_of(xx * wide + h * cw, cw), cw)]
-
     def wx_copy(m, h):
-        return remote(own_cols(m, h, 1 - x), piece(m, h, fs), wx_s.at[m, h], w_r.at[m, h, fs], x_next)
-
-    def wz_copy(m, h, f, way, own=False):
-        src = own_cols(m, h, x) if own else piece(m, h, f)
-        return remote(src, piece(m, h, f), wz_s.at[way, m, h, f], w_r.at[m, h, f], left if way else right)
+        return remote(own_w[m].at[:, columns_at(1 - x, h)], piece(m, h, fs), wx_s, w_r.at[m, h, fs], x_next)
+
+    def wz_copy(m, h, f, way):
+        return remote(piece(m, h, f), piece(m, h, f), wz_s.at[way, m, h], w_r.at[m, h, f], left if way else right)
 
     def w_got(m, h, f):
         wz_copy(m, h, f, 0).wait_recv()
 
-    def spread(m, h, f, own=False):
+    def spread(m, h, f):
         @pl.when(z < last)
         def _():
-            wz_copy(m, h, f, 0, own).start()
+            wz_copy(m, h, f, 0).start()
 
         @pl.when(z > 0)
         def _():
-            wz_copy(m, h, f, 1, own).start()
+            wz_copy(m, h, f, 1).start()
 
     def from_x(h, ms=(0, 1)):
         for m in ms:
@@ -430,38 +453,38 @@
                     w_got(m, h, (z + d) * 2 + p)
                     wz_copy(m, h, (z + d) * 2 + p, 1).start()
 
-    def settle(h, m):
+    def settle(h, m, lo, hi):
         @pl.when((z == 0) | (z == last))
         def _():
-            @pl.loop(1, z_size)
+            @pl.loop(lo, hi)
             def _(d):
                 for p in range(2):
-                    w_got(m, h, (z + d) % z_size * 2 + p)
-
-    cut_t = rows_dev * 3 // 4 // 16 * 16
-    moves = (
-        (x, y, 0, rows_dev, x_next),
-        (x, y, 0, rows_dev, y_next),
-        (1 - x, y, 0, cut_t, y_next),
-        (x, 1 - y, cut_t, rows_dev - cut_t, x_next),
-        (x, y, 0, rows_dev, mate),
-        (1 - x, y, 0, rows_dev, mate),
-        (x, 1 - y, 0, rows_dev, mate),
-        (1 - x, 1 - y, 0, cut_t, mate),
-        (1 - x, 1 - y, cut_t, rows_dev - cut_t, mate),
-    )
-
-    def block_at(xx, yy, cc):
-        return ((xx * 2 + yy) * 2 + cc) * rows_dev
-
-    def t_copy(a, k, own=False):
-        xx, yy, lo, count, to = moves[k]
+                    w_got(m, h, jnp.where(z == 0, d, last - d) * 2 + p)
+
+    def moves(cut_t):
+        return (
+            (x, y, 0, rows_dev, x_next, 0),
+            (x, y, 0, rows_dev, y_next, 1),
+            (1 - x, y, 0, cut_t, y_next, 2),
+            (x, 1 - y, cut_t, rows_dev - cut_t, x_next, 3),
+            (x, y, 0, rows_dev, mate, 4),
+            (1 - x, y, 0, rows_dev, mate, 4),
+            (x, 1 - y, 0, rows_dev, mate, 4),
+            (1 - x, 1 - y, 0, cut_t, mate, 5),
+            (1 - x, 1 - y, cut_t, rows_dev - cut_t, mate, 5),
+        )
+
+    cuts = tuple(rows_dev * part // 4 // 16 * 16 for part in (3, 3, 2))
+
+    def t_copy(a, k):
+        xx, yy, lo, count, to, got = moves(cuts[a])[k]
         there = tok.at[a, rows_at(block_at(xx, yy, c) + lo, count), :]
-        return remote(own_t[a] if own else there, there, t_s.at[a, k], t_r.at[a, k], to)
+        return remote(there, there, t_s.at[a], t_r.at[a, got], to)
 
     def t_first(a):
+        load_t(a).wait()
         for k in (0, 1, 4):
-            t_copy(a, k, True).start()
+            t_copy(a, k).start()
 
     def t_pass_y(a):
         t_copy(a, 1).wait_recv()
@@ -479,17 +502,13 @@
         t_copy(a, 3).wait_recv()
         t_copy(a, 8).start()
 
-    def t_wait(a, kinds):
-        for k in kinds:
-            t_copy(a, k).wait_recv()
-
-    def put(dst, dst_row, src, columns, count):
-        step = math.gcd(count, 64)
-
-        @pl.loop(0, count // step)
-        def _(i):
-            o = pl.multiple_of(i * step, step)
-            dst[pl.ds(pl.multiple_of(dst_row + o, step), step), :] = src[pl.ds(o, step), columns]
+    def t_mate(a):
+        there = tok.at[a, pl.ds(0, 3 * rows_dev), :]
+        remote(there, there, t_s.at[a], t_r.at[a, 4], mate).wait_recv()
+
+    def t_mate_diagonal(a):
+        there = tok.at[a, pl.ds(0, rows_dev), :]
+        remote(there, there, t_s.at[a], t_r.at[a, 5], mate).wait_recv()
 
     def chip_at(i):
         return (((x + i % 2) % 2) * 2 + (y + i // 2) % 2) * chip_rows
@@ -515,10 +534,14 @@
         grads[m, h, o, :] = lax.dot_general(
             tok[m, :, o], hid[m, h], (((0,), (0,)), ((), ())), preferred_element_type=F32).astype(BF16)
 
-    def g_copy(m, h, d, way):
-        src = grads.at[m, h, rows_at(d * zrows, zrows), :]
+    def half_at(d, half):
+        return d * zrows + (x + 1 - half) % 2 * blk
+
+    def g_copy(m, h, d, way, half):
+        src = grads.at[m, h, rows_at(half_at(d, half), blk), :]
         to = {"fs": ((z + z_size + 1 - 2 * way) % z_size) * 2 + x, "tp": tp}
-        return remote(src, gbuf.at[way, m, h, d], g_s.at[way, m, h, d], g_r.at[way, m, h, d], to)
+        slot = d + 1 - way
+        return remote(src, gbuf.at[m, h, slot, half], g_s.at[way, m, h], g_r.at[m, h, slot, half], to)
 
     def terms(h, lo, hi):
         @pl.loop(lo, hi)
@@ -531,7 +554,8 @@
 
                     @pl.when(z == 0)
                     def _():
-                        g_copy(m, h, last - k, 0).start()
+                        for half in range(2):
+                            g_copy(m, h, last - k, 0, half).start()
 
             @pl.when(k < z)
             def _():
@@ -541,21 +565,22 @@
 
                     @pl.when(z == last)
                     def _():
-                        g_copy(m, h, k, 1).start()
+                        for half in range(2):
+                            g_copy(m, h, k, 1, half).start()
 
     def own_terms(h):
         @pl.loop(0, 2)
         def _(m):
             term(m, h, z)
 
-    def add_rows(dst, dst_row, src, count):
+    def add_rows(dst, dst_row, src, count, columns=slice(None)):
         step = math.gcd(count, 32)
 
         @pl.loop(0, count // step)
         def _(i):
             o = pl.multiple_of(i * step, step)
             at = pl.ds(pl.multiple_of(dst_row + o, math.gcd(step, 16)), step)
-            dst[at, :] = (dst[at, :].astype(F32) + src[pl.ds(o, step), :].astype(F32)).astype(BF16)
+            dst[at, columns] = (dst[at, columns].astype(F32) + src[pl.ds(o, step), columns].astype(F32)).astype(BF16)
 
     side = 2 * z // z_size
 
@@ -567,66 +592,75 @@
 
         @pl.when((beyond > 0) & (behind > 0))
         def _():
-            g_copy(m, h, d, way).wait_recv()
-            add_rows(grads.at[m, h], d * zrows, gbuf.at[way, m, h, d], zrows)
-            g_copy(m, h, d, way).start()
+            for half in range(2):
+                g_copy(m, h, d, way, half).wait_recv()
+                add_rows(grads.at[m, h], half_at(d, half), gbuf.at[m, h, d + 1 - way, half], blk)
+                g_copy(m, h, d, way, half).start()
 
     outs = (up_out, down_out)
 
     def f_copy(m, h):
-        return remote(fin.at[m, h], xbuf.at[m, h], f_s.at[m, h], f_r.at[m, h], x_next)
-
-    def total(m, h, xx, dst, columns, sources):
+        return remote(fin.at[m, h], xbuf.at[m, h], f_s, f_r.at[m, h], x_next)
+
+    def total(m, h, half, sources):
         step = math.gcd(blk, 32)
 
         @pl.loop(0, blk // step)
         def _(i):
             o = pl.multiple_of(i * step, step)
-            at = pl.ds(pl.multiple_of(xx * blk + o, step), step)
-            got = grads[m, h, pl.ds(pl.multiple_of(z * zrows + xx * blk + o, step), step), :].astype(F32)
+            at = pl.ds(o, step)
+            got = grads[m, h, pl.ds(pl.multiple_of(half_at(z, half) + o, step), step), :].astype(F32)
             for src in sources:
-                got += gbuf[src, m, h, z, at, :].astype(F32)
-            dst[pl.ds(o, step), columns] = got.astype(BF16)
-
-    def finish(h, ms=(0, 1)):
-        mine = pl.ds(pl.multiple_of(x * wide + h * cw, cw), cw)
-        for m in ms:
+                got += gbuf[m, h, z + 1 - src, half, at, :].astype(F32)
+            if half:
+                sums[m, at, columns_at(x, h)] += got * factor
+            else:
+                fin[m, h, at, :] = got.astype(BF16)
+
+    def store_sum(m, h, xx):
+        there = columns_at(xx, h)
+        return pltpu.make_async_copy(sums.at[m, :, there], outs[m].at[:, there], o_s.at[m])
+
+    def finish(h, m):
+        for half in range(2):
             @pl.when(z > 0)
             def _():
-                g_copy(m, h, z, 0).wait_recv()
+                g_copy(m, h, z, 0, half).wait_recv()
 
             @pl.when(z < last)
             def _():
-                g_copy(m, h, z, 1).wait_recv()
+                g_copy(m, h, z, 1, half).wait_recv()
 
             for case, sources in ((z == 0, (1,)), (z == last, (0,)), ((z > 0) & (z < last), (0, 1))):
                 @pl.when(case)
                 def _():
-                    total(m, h, 1 - x, fin.at[m, h], slice(None), sources)
-
-            f_copy(m, h).start()
-            for case, sources in ((z == 0, (1,)), (z == last, (0,)), ((z > 0) & (z < last), (0, 1))):
-                @pl.when(case)
-                def _():
-                    total(m, h, x, outs[m], mine, sources)
-
-    def finish_x(h):
-        theirs = pl.ds(pl.multiple_of((1 - x) * wide + h * cw, cw), cw)
+                    total(m, h, half, sources)
+
+            (store_sum(m, h, x) if half else f_copy(m, h)).start()
+
+    def finish_x(h, m):
+        f_copy(m, h).wait_recv()
         step = math.gcd(blk, 32)
-        for m in range(2):
-            f_copy(m, h).wait_recv()
-
-            @pl.loop(0, blk // step)
-            def _(i):
-                o = pl.ds(pl.multiple_of(i * step, step), step)
-                outs[m][o, theirs] = xbuf[m, h, o, :]
-
-    tile = math.gcd(depth, 256)
-
-    def partial(a, k, w):
-        @pl.loop(0, depth // tile)
+
+        @pl.loop(0, blk // step)
+        def _(i):
+            at = pl.ds(pl.multiple_of(i * step, step), step)
+            sums[m, at, columns_at(1 - x, h)] += xbuf[m, h, at, :].astype(F32) * factor
+
+        store_sum(m, h, 1 - x).start()
+
+    span = 2 * blk
+    tile = math.gcd(span, 256)
+
+    def span_at(i):
+        return rows_at(((1 - side) * i + side * (last - i)) * span, span)
+
+    def partial(a, k, w, i):
+        first = ((1 - side) * i + side * (last - i)) * span
+
+        @pl.loop(0, span // tile)
         def _(j):
-            o = pl.ds(pl.multiple_of(j * tile, tile), tile)
+            o = rows_at(first + j * tile, tile)
             got = None
             for h in range(chunks):
                 one = lax.dot_general(hid[k, h], wts[w, h, o, :], (((1,), (1,)), ((), ())),
@@ -634,13 +668,12 @@
                 got = one if got is None else got + one
             part[a, :, o] = got.astype(BF16)
 
-    def d_copy(a, q):
-        return remote(part.at[a, rows_at(q * chip_rows + (1 - c) * rows_dev, rows_dev), :], dbuf.at[a, q],
-                      d_s.at[a, q], d_r.at[a, q], mate)
-
-    def d_start(a):
         for q in range(4):
-            d_copy(a, q).start()
+            d_copy(a, q, i).start()
+
+    def d_copy(a, q, i):
+        return remote(part.at[a, rows_at(q * chip_rows + (1 - c) * rows_dev, rows_dev), span_at(i)],
+                      dbuf.at[a, q, :, span_at(i)], d_s.at[a], d_r.at[a, i], mate)
 
     cut_q = rows_dev * 3 // 8 // 16 * 16
     low, high = (0, cut_q), (cut_q, rows_dev - cut_q)
@@ -653,29 +686,43 @@
         (1 - x, y, high, qb, 2, x_next),
     )
 
-    def q_copy(a, k):
+    def q_copy(a, k, i):
         xx, yy, (lo, count), buf, slot, to = hops[k]
-        return remote(part.at[a, rows_at(block_at(xx, yy, c) + lo, count), :], buf.at[a, slot],
-                      q_s.at[a, k], q_r.at[a, k], to)
-
-    def q_first(a):
+        return remote(part.at[a, rows_at(block_at(xx, yy, c) + lo, count), span_at(i)],
+                      buf.at[a, slot, :, span_at(i)], q_s.at[a], q_r.at[a, k // 2, i] if k in (1, 3) else q_l.at[a], to)
+
+    def q_first(a, i):
+        there = dbuf.at[a, :, :, span_at(i)]
+        remote(there, there, d_s.at[a], d_r.at[a, i], mate).wait_recv()
         for q in range(4):
-            d_copy(a, q).wait_recv()
-            add_rows(part.at[a], q * chip_rows + c * rows_dev, dbuf.at[a, q], rows_dev)
-        for k in range(4):
-            q_copy(a, k).start()
-
-    def q_second(a):
-        q_copy(a, 1).wait_recv()
-        add_rows(part.at[a], block_at(x, 1 - y, c), qa.at[a, 1], cut_q)
-        q_copy(a, 4).start()
-        q_copy(a, 3).wait_recv()
-        add_rows(part.at[a], block_at(1 - x, y, c) + cut_q, qb.at[a, 1], rows_dev - cut_q)
-        q_copy(a, 5).start()
-
-    def q_last(a, out):
-        for k in (0, 4, 2, 5):
-            q_copy(a, k).wait_recv()
+            add_rows(part.at[a], q * chip_rows + c * rows_dev, dbuf.at[a, q], rows_dev, span_at(i))
+        for k in (1, 3):
+            q_copy(a, k, i).start()
+
+    def q_rest(a, i):
+        for k in (0, 2):
+            q_copy(a, k, i).start()
+
+    def q_second(a, i):
+        q_copy(a, 1, i).wait_recv()
+        add_rows(part.at[a], block_at(x, 1 - y, c), qa.at[a, 1], cut_q, span_at(i))
+        q_copy(a, 4, i).start()
+        q_copy(a, 3, i).wait_recv()
+        add_rows(part.at[a], block_at(1 - x, y, c) + cut_q, qb.at[a, 1], rows_dev - cut_q, span_at(i))
+        q_copy(a, 5, i).start()
+
+    def over(lo, hi, *calls):
+        @pl.loop(lo, hi)
+        def _(i):
+            for call in calls:
+                call(i)
+
+    def store_out(a):
+        return pltpu.make_async_copy(stage.at[a], (earlier_out, later_out)[a], o_s.at[2 + a])
+
+    def q_last(a):
+        there = part.at[a, pl.ds(0, 2 * rows_dev), :]
+        remote(there, there, q_s.at[a], q_l.at[a], x_next).wait_recv()
         for (lo, count), buf in ((low, qa), (high, qb)):
             step = math.gcd(count, 16)
 
@@ -684,24 +731,21 @@
                 o = pl.multiple_of(i * step, step)
                 at = pl.ds(o, step)
                 own = pl.ds(pl.multiple_of(block_at(x, y, c) + lo + o, step), step)
-                out[pl.ds(pl.multiple_of(lo + o, step), step), :] = (
+                stage[a, pl.ds(pl.multiple_of(lo + o, step), step), :] = (
                     part[a, own, :].astype(F32) + buf[a, 0, at, :].astype(F32) + buf[a, 2, at, :].astype(F32)
                 ).astype(BF16)
+
+        store_out(a).start()
 
     for m in range(2):
         wx_copy(m, 0).start()
     for m in range(2):
-        spread(m, 0, fs, True)
+        load_w(m, 0).wait()
+        spread(m, 0, fs)
     t_first(0)
     t_first(1)
     for m in range(2):
         wx_copy(m, 1).start()
-    for m in range(2):
-        for h in range(chunks):
-            cols = pl.ds(pl.multiple_of(x * wide + h * cw, cw), cw)
-            put(wts.at[m, h], fs * blk, own_w[m], cols, blk)
-    for a in range(3):
-        put(tok.at[a], block_at(x, y, c), own_t[a], slice(None), rows_dev)
     from_x(0)
     relay(0, 1)
     t_pass_y(0)
@@ -710,142 +754,176 @@
     t_pass_y(1)
     t_pass_x(1)
     for m in range(2):
-        spread(m, 1, fs, True)
+        load_w(m, 1).wait()
+        spread(m, 1, fs)
     t_first(2)
-    settle(0, 0)
-    settle(0, 1)
+    for m in range(2):
+        settle(0, m, 1, z_size)
     for a in range(2):
-        t_wait(a, (4, 5, 6))
+        t_mate(a)
     earlier_hidden(0, 0, 3)
     from_x(1)
     t_diagonal(0)
     relay(1, 1, (0,))
     t_diagonal(1)
     for a in range(2):
-        t_wait(a, (7, 8))
+        t_mate_diagonal(a)
     earlier_hidden(0, 3, 4)
     terms(0, 0, last)
     own_terms(0)
-    t_pass_y(2)
     relay(1, 1, (1,), (0,))
     relay(1, 2, (0,), (0,))
+    t_pass_y(2)
     reduce_step(0, 0, 0, True)
-    t_pass_x(2)
     relay(1, 2, (1,), (0,))
     relay(1, 1, (1,), (1,))
     relay(1, 2, (0,), (1,))
+    t_pass_x(2)
     reduce_step(0, 0, 1, True)
     relay(1, 2, (1,), (1,))
     reduce_step(0, 0, 0, False)
     t_diagonal(2)
-    settle(1, 0)
-    t_wait(2, (4, 5, 6, 7, 8))
+    settle(1, 0, 1, z_size)
+    t_mate(2)
+    t_mate_diagonal(2)
     later_hidden(0)
     later_hidden(1)
     reduce_step(0, 1, 0, True)
     reduce_step(0, 0, 1, False)
-    settle(1, 1)
-    partial(1, 2, 1)
-    d_start(1)
+    settle(1, 1, 1, last)
+    over(0, last, lambda i: partial(1, 2, 1, i))
+    settle(1, 1, last, z_size)
+    partial(1, 2, 1, last)
+    over(0, last, lambda i: q_first(1, i))
     earlier_hidden(1, 0, 4)
     reduce_step(0, 1, 1, True)
     terms(1, 0, 1)
-    q_first(1)
+    q_first(1, last)
+    over(0, z_size, lambda i: q_rest(1, i))
     terms(1, 1, last)
     own_terms(1)
-    partial(0, 0, 0)
-    d_start(0)
-    finish(0, (0,))
-    finish(0, (1,))
-    q_first(0)
+    partial(0, 0, 0, 0)
+    over(1, z_size, lambda i: partial(0, 0, 0, i), lambda i: q_first(0, i - 1))
+    for m in range(2):
+        totals[m].wait()
+        finish(0, m)
+    q_first(0, last)
+    over(0, z_size, lambda i: q_second(1, i))
+    over(0, z_size, lambda i: q_rest(0, i))
     reduce_step(1, 0, 0, True)
     reduce_step(1, 0, 1, True)
-    q_second(1)
     reduce_step(1, 0, 0, False)
-    finish_x(0)
+    over(0, z_size, lambda i: q_second(0, i))
+    finish_x(0, 0)
+    finish_x(0, 1)
     reduce_step(1, 1, 0, True)
     reduce_step(1, 0, 1, False)
     reduce_step(1, 1, 1, True)
-    q_second(0)
-    q_last(1, later_out)
-    q_last(0, earlier_out)
-    finish(1, (0,))
-    finish(1, (1,))
-    finish_x(1)
-
+    finish(1, 0)
+    q_last(1)
+    finish(1, 1)
+    q_last(0)
+    finish_x(1, 0)
+    finish_x(1, 1)
+
+    def sent(ref, semaphore):
+        remote(ref, ref, semaphore, f_r.at[0, 0], mate).wait_send()
+
+    four = wts.at[0, 0, pl.ds(0, 2 * chunks * blk), :]
+    sent(four, wx_s)
+    sent(four, f_s)
     for m in range(2):
+        pltpu.make_async_copy(outs[m], outs[m], o_s.at[m]).wait()
         for h in range(chunks):
-            wx_copy(m, h).wait_send()
-            f_copy(m, h).wait_send()
-
-            @pl.loop(0, n)
-            def _(f):
-                @pl.when((f // 2 <= z) & (z < last))
-                def _():
-                    wz_copy(m, h, f, 0).wait_send()
-
-                @pl.when((f // 2 >= z) & (z > 0))
-                def _():
-                    wz_copy(m, h, f, 1).wait_send()
-
-            @pl.loop(0, z_size)
-            def _(d):
-                @pl.when(d > z)
-                def _():
-                    g_copy(m, h, d, 0).wait_send()
-
-                @pl.when(d < z)
-                def _():
-                    g_copy(m, h, d, 1).wait_send()
+            for way in range(2):
+                for hops_left in range(1, z_size):
+                    @pl.when((last - z if way == 0 else z) == hops_left)
+                    def _():
+                        sent(wts.at[m, h, pl.ds(0, (z_size - hops_left) * zrows), :], wz_s.at[way, m, h])
+                        sent(grads.at[m, h, pl.ds(0, hops_left * zrows), :], g_s.at[way, m, h])
     for a in range(3):
-        for k in range(9):
-            t_copy(a, k).wait_send()
+        sent(tok.at[a, pl.ds(0, 7 * rows_dev), :], t_s.at[a])
     for a in range(2):
-        for q in range(4):
-            d_copy(a, q).wait_send()
-        for k in range(6):
-            q_copy(a, k).wait_send()
-
-
-def plane_call(n, m, *args):
+        store_out(a).wait()
+        sent(part.at[a, pl.ds(0, 4 * rows_dev), :], d_s.at[a])
+        sent(part.at[a, pl.ds(0, 3 * rows_dev), :], q_s.at[a])
+
+
+def plane_call(n, factor, *args):
     rows_dev, depth = args[0].shape
     blk, width = args[3].shape
     z_size, chunks, rows = n // 2, 2, rows_dev * 8
     cw = width // 2 // chunks
     cut_q = rows_dev * 3 // 8 // 16 * 16
     dma = pltpu.SemaphoreType.DMA
-    vmem = pl.BlockSpec(memory_space=pltpu.VMEM)
+    hbm = pl.BlockSpec(memory_space=pltpu.HBM)
     return pl.pallas_call(
-        functools.partial(plane_kernel, n, chunks),
+        functools.partial(plane_kernel, n, chunks, factor),
         out_shape=(
             jax.ShapeDtypeStruct((rows_dev, depth), BF16),
             jax.ShapeDtypeStruct((rows_dev, depth), BF16),
-            jax.ShapeDtypeStruct((blk, width), BF16),
-            jax.ShapeDtypeStruct((blk, width), BF16),
+            jax.ShapeDtypeStruct((blk, width), F32),
+            jax.ShapeDtypeStruct((blk, width), F32),
         ),
-        in_specs=[vmem] * 5,
-        out_specs=(vmem,) * 4,
+        in_specs=[hbm] * 7,
+        out_specs=(hbm,) * 4,
         scratch_shapes=[
             pltpu.VMEM((3, rows, depth), BF16),
             pltpu.VMEM((2, chunks, depth, cw), BF16),
             pltpu.VMEM((3, chunks, rows, cw), BF16),
             pltpu.VMEM((2, chunks, depth, cw), BF16),
-            pltpu.VMEM((2, 2, chunks, z_size, 2 * blk, cw), BF16),
+            pltpu.VMEM((2, chunks, z_size + 1, 2, blk, cw), BF16),
             pltpu.VMEM((2, chunks, blk, cw), BF16),
             pltpu.VMEM((2, chunks, blk, cw), BF16),
             pltpu.VMEM((2, rows, depth), BF16),
             pltpu.VMEM((2, 4, rows_dev, depth), BF16),
             pltpu.VMEM((2, 3, cut_q, depth), BF16),
             pltpu.VMEM((2, 3, rows_dev - cut_q, depth), BF16),
-            dma((3, 9)), dma((3, 9)), dma((2, chunks)), dma((2, 2, chunks, n)), dma((2, chunks, n)),
-            dma((2, 2, chunks, z_size)), dma((2, 2, chunks, z_size)), dma((2, chunks)), dma((2, chunks)),
-            dma((2, 4)), dma((2, 4)), dma((2, 6)), dma((2, 6)),
+            pltpu.VMEM((2, rows_dev, depth), BF16),
+            pltpu.VMEM((2, blk, width), F32),
+            dma((2 * chunks + 5,)), dma((4,)), dma((3,)), dma((3, 6)), dma, dma((2, 2, chunks)), dma((2, chunks, n)),
+            dma((2, 2, chunks)), dma((2, chunks, z_size + 1, 2)), dma, dma((2, chunks)),
+            dma((2,)), dma((2, z_size)), dma((2,)), dma((2, 2, z_size)), dma((2,)),
         ],
         compiler_params=pltpu.CompilerParams(
             collective_id=0, has_side_effects=True, vmem_limit_bytes=67043328
         ),
         name="feed_forward_planes",
     )(*args)
+
+
+def hand_on_kernel(*refs):
+    count = (len(refs) - 2) // 3
+    ins, outs, held, in_s, out_s = refs[:count], refs[count:2 * count], refs[2 * count:-2], refs[-2], refs[-1]
+    loads, stores = [], []
+    for a, (src, kept, dst) in enumerate(zip(ins, held, outs)):
+        half = src.shape[0] // 2
+        for i in range(2):
+            o = pl.ds(i * half, half)
+            loads.append(pltpu.make_async_copy(src.at[o, :], kept.at[o, :], in_s.at[a, i]))
+            stores.append(pltpu.make_async_copy(kept.at[o, :], dst.at[o, :], out_s.at[a, i]))
+    for load in loads:
+        load.start()
+    for load, store in zip(loads, stores):
+        load.wait()
+        store.start()
+    for store in stores:
+        store.wait()
+
+
+def hand_on(*arrays):
+    count = len(arrays)
+    hbm = pl.BlockSpec(memory_space=pltpu.HBM)
+    return pl.pallas_call(
+        hand_on_kernel,
+        out_shape=tuple(jax.ShapeDtypeStruct(a.shape, a.dtype) for a in arrays),
+        in_specs=[hbm] * count,
+        out_specs=(hbm,) * count,
+        scratch_shapes=[*(pltpu.VMEM(a.shape, a.dtype) for a in arrays),
+                        pltpu.SemaphoreType.DMA((count, 2)), pltpu.SemaphoreType.DMA((count, 2))],
+        compiler_params=pltpu.CompilerParams(vmem_limit_bytes=67043328),
+        name="feed_forward_results",
+    )(*arrays)
 
 
 def ring_call(n, m, *args):
@@ -892,8 +970,10 @@
     factor = 1.0 / math.sqrt(rows * n)
     width = up_weight.shape[1]
     planar = columns_of(n) == 2 and n == 8 and m == 4 and width % 1024 == 0 and rows % 512 == 0
-    later_out, earlier_grad, up_term, down_term = (plane_call if planar else ring_call)(
-        n, m, later_rows, earlier_rows, cotangent, up_weight, down_weight)
+    planes = (later_rows, earlier_rows, cotangent, up_weight, down_weight)
+    if planar:
+        return tuple(hand_on(*plane_call(n, factor, *planes, up_total, down_total)))
+    later_out, earlier_grad, up_term, down_term = ring_call(n, m, *planes)
     up_updated = up_total + up_term.astype(F32) * factor
     down_updated = down_total + down_term.astype(F32) * factor
     return later_out, earlier_grad, up_updated, down_updated

time: 142 us -> 129 us (0.908)
  Pallas kernels: 135 us -> 127 us
  other arithmetic: 3.68 us -> 0 us
  local copies, waits for them, and re-layouts: 2.03 us -> 0 us
    pallas_call x1 -> x2, Pallas kernels: 135 us -> 127 us  [the longest x1 124 us: plane_call(): pl.pallas_call(functools.partial(plane_kernel, n, chunks, factor), out_sh...]
    add x1 -> x0, other arithmetic: 3.68 us -> none  [body(): down_updated = down_total + down_term.astype(F32) * factor]
    unnamed x6 -> x0, local copies, waits for them, and re-layouts: 2.03 us -> none
where the time goes in v3:
time: 129 us; the launch traced here: 128 us
  Pallas kernels  127 us (98%)
    pallas_call x1, Pallas kernels, plane_call(): pl.pallas_call(functools.partial(plane_kernel, n, chunks, factor), out_sh...  124 us
    pallas_call x1, Pallas kernels, hand_on(): pl.pallas_call(hand_on_kernel, out_shape=tuple((jax.ShapeDtypeStruct(a.sh...  2.81 us

profile of v3, /device:TPU:0, one launch (start us, length us, event | category | flops | bytes accessed | tf_op | source)
XLA Modules:
  0.0 127.6 jit_solution(15836193739066613660)
XLA Ops:
  0.6 124.1 %feed_forward_planes.1 = (bf16[128,2048]{1,0:T(8,128)(2,1)}, bf16[128,2048]{1,0:T(8,128)(2,1)}, f32[256,1024]{1,0:T(8,128)}, f32[256,1024]{1,0:T(8,128)}) custom-call(bf16[128,2048]{1,0:T(8,128)(2,1)} %later_ref.1, bf16[128,2048]{1,0:T(8,128)(2,1)} %earlier_ref.1, bf16[128,2048]{1,0:T(8,128)(2,1)} %cot_ref.1, bf16[256,1024]{1,0:T(8,128)(2,1)} %up_ref.1, ...), custom_call_target="tpu_custom_call" | custom-call | tf_op jit(solution)/shard_map/feed_forward_planes/pallas_call | solution.py:860
  124.8 2.8 %feed_forward_results.1 = (bf16[128,2048]{1,0:T(8,128)(2,1)}, bf16[128,2048]{1,0:T(8,128)(2,1)}, f32[256,1024]{1,0:T(8,128)}, f32[256,1024]{1,0:T(8,128)}) custom-call(bf16[128,2048]{1,0:T(8,128)(2,1)} %get-tuple-element.8.refs_0_, bf16[128,2048]{1,0:T(8,128)(2,1)} %get-tuple-element.9.refs_1_, f32[256,1024]{1,0:T(8,128)} %get-tuple-element.10.refs_2_, ...), custom_call_target="tpu_custom_call" | custom-call | tf_op jit(solution)/shard_map/feed_forward_results/pallas_call | solution.py:917

commit v4 on v3

--- a/solution.py
+++ b/solution.py
@@ -354,7 +354,7 @@
 def plane_kernel(n, chunks, factor,
                  later_ref, earlier_ref, cot_ref, up_ref, down_ref, up_total, down_total,
                  later_out, earlier_out, up_out, down_out,
-                 tok, wts, hid, grads, gbuf, fin, xbuf, part, dbuf, qa, qb, stage, sums,
+                 tok, wts, act, hid, grads, gbuf, fin, xbuf, part, dbuf, qa, qb, stage, sums,
                  l_s, o_s, t_s, t_r, wx_s, wz_s, w_r, g_s, g_r, f_s, f_r, d_s, d_r, q_s, q_r, q_l):
     rows_dev, depth = later_ref.shape
     blk, width = up_ref.shape
@@ -364,6 +364,8 @@
     fs, tp = lax.axis_index("fs"), lax.axis_index("tp")
     z, x, y, c = fs // 2, fs % 2, tp // 2, tp % 2
     last = z_size - 1
+    side = 2 * z // z_size
+    span = 2 * blk
 
     right = {"fs": ((z + 1) % z_size) * 2 + x, "tp": tp}
     left = {"fs": ((z + last) % z_size) * 2 + x, "tp": tp}
@@ -433,10 +435,20 @@
         def _():
             wz_copy(m, h, f, 1).start()
 
+    def spread_at(m, h, f, ends):
+        @pl.when((z == 0) | (z == last) if ends else (z > 0) & (z < last))
+        def _():
+            spread(m, h, f)
+
     def from_x(h, ms=(0, 1)):
         for m in ms:
             w_got(m, h, z * 2 + 1 - x)
             spread(m, h, z * 2 + 1 - x)
+
+    def from_x_at(h, ms, ends):
+        @pl.when((z == 0) | (z == last) if ends else (z > 0) & (z < last))
+        def _():
+            from_x(h, ms)
 
     def relay(h, d, columns=(0, 1), ms=(0, 1)):
         for m in ms:
@@ -474,58 +486,77 @@
             (1 - x, 1 - y, cut_t, rows_dev - cut_t, mate, 5),
         )
 
-    cuts = tuple(rows_dev * part // 4 // 16 * 16 for part in (3, 3, 2))
-
-    def t_copy(a, k):
-        xx, yy, lo, count, to, got = moves(cuts[a])[k]
-        there = tok.at[a, rows_at(block_at(xx, yy, c) + lo, count), :]
-        return remote(there, there, t_s.at[a], t_r.at[a, got], to)
-
-    def t_first(a):
-        load_t(a).wait()
+    cuts = tuple(rows_dev * part // 8 // 16 * 16 for part in (7, 5, 4))
+
+    def facing(i):
+        return (1 - side) * (last - i) + side * i
+
+    def t_ref(a, start, count, u):
+        columns = slice(None) if u is None else rows_at(facing(u) * span, span)
+        return tok.at[a, rows_at(start, count), columns]
+
+    def t_got(a, k, u):
+        if a == 2:
+            return t_r.at[moves(0)[k][-1]]
+        return t_r.at[6 + (a * 5 + min(k, 4)) * z_size + (0 if a == 0 and k > 3 else u)]
+
+    def t_copy(a, k, u=None):
+        xx, yy, lo, count, to, _ = moves(cuts[a])[k]
+        there = t_ref(a, block_at(xx, yy, c) + lo, count, u)
+        return remote(there, there, t_s.at[a], t_got(a, k, u), to)
+
+    def t_own(a, u=None):
         for k in (0, 1, 4):
-            t_copy(a, k).start()
-
-    def t_pass_y(a):
-        t_copy(a, 1).wait_recv()
-        t_copy(a, 3).start()
-        t_copy(a, 6).start()
-
-    def t_pass_x(a):
-        t_copy(a, 0).wait_recv()
-        t_copy(a, 2).start()
-        t_copy(a, 5).start()
-
-    def t_diagonal(a):
-        t_copy(a, 2).wait_recv()
-        t_copy(a, 7).start()
-        t_copy(a, 3).wait_recv()
-        t_copy(a, 8).start()
-
-    def t_mate(a):
-        there = tok.at[a, pl.ds(0, 3 * rows_dev), :]
-        remote(there, there, t_s.at[a], t_r.at[a, 4], mate).wait_recv()
-
-    def t_mate_diagonal(a):
-        there = tok.at[a, pl.ds(0, rows_dev), :]
-        remote(there, there, t_s.at[a], t_r.at[a, 5], mate).wait_recv()
+            t_copy(a, k, u).start()
+
+    def t_pass(a, u=None):
+        t_copy(a, 1, u).wait_recv()
+        t_copy(a, 3, u).start()
+        t_copy(a, 6, u).start()
+        t_copy(a, 0, u).wait_recv()
+        t_copy(a, 2, u).start()
+        t_copy(a, 5, u).start()
+
+    def t_diagonal(a, u=None):
+        t_copy(a, 2, u).wait_recv()
+        t_copy(a, 7, u).start()
+        t_copy(a, 3, u).wait_recv()
+        t_copy(a, 8, u).start()
+
+    def t_mate(a, u=None):
+        there = t_ref(a, 0, 4 * rows_dev, u)
+        remote(there, there, t_s.at[a], t_got(a, 4, u), mate).wait_recv()
+
+    def t_mate_blocks():
+        there = t_ref(2, 0, 3 * rows_dev, None)
+        remote(there, there, t_s.at[2], t_r.at[4], mate).wait_recv()
+
+    def t_mate_diagonal():
+        there = t_ref(2, 0, rows_dev, None)
+        remote(there, there, t_s.at[2], t_r.at[5], mate).wait_recv()
+
+    def earlier_hidden(h):
+        @pl.loop(0, 4)
+        def _(i):
+            o = rows_at(i * chip_rows, chip_rows)
+            relu = jnp.maximum(jnp.dot(tok[0, o, :], wts[0, h], preferred_element_type=F32), 0.0)
+            act[o, :] = relu
+            hid[1, h, o, :] = (relu * relu).astype(BF16)
+
+    def earlier_pre_grad(h):
+        @pl.loop(0, 4)
+        def _(i):
+            o = rows_at(i * chip_rows, chip_rows)
+            got = jnp.dot(tok[1, o, :], wts[1, h], preferred_element_type=F32)
+            hid[0, h, o, :] = (2.0 * act[o, :] * got).astype(BF16)
 
     def chip_at(i):
         return (((x + i % 2) % 2) * 2 + (y + i // 2) % 2) * chip_rows
 
-    def earlier_hidden(h, lo, hi):
+    def later_hidden(h, lo, hi):
         @pl.loop(lo, hi)
         def _(i):
             o = rows_at(chip_at(i), chip_rows)
-            relu = jnp.maximum(jnp.dot(tok[0, o, :], wts[0, h], preferred_element_type=F32), 0.0)
-            got = jnp.dot(tok[1, o, :], wts[1, h], preferred_element_type=F32)
-            hid[0, h, o, :] = (2.0 * relu * got).astype(BF16)
-            hid[1, h, o, :] = (relu * relu).astype(BF16)
-
-    def later_hidden(h):
-        @pl.loop(0, 4)
-        def _(i):
-            o = rows_at(i * chip_rows, chip_rows)
             relu = jnp.maximum(jnp.dot(tok[2, o, :], wts[0, h], preferred_element_type=F32), 0.0)
             hid[2, h, o, :] = (relu * relu).astype(BF16)
 
@@ -543,35 +574,14 @@
         slot = d + 1 - way
         return remote(src, gbuf.at[m, h, slot, half], g_s.at[way, m, h], g_r.at[m, h, slot, half], to)
 
-    def terms(h, lo, hi):
-        @pl.loop(lo, hi)
-        def _(k):
-            @pl.when(last - k > z)
-            def _():
-                @pl.loop(0, 2)
-                def _(m):
-                    term(m, h, last - k)
-
-                    @pl.when(z == 0)
-                    def _():
-                        for half in range(2):
-                            g_copy(m, h, last - k, 0, half).start()
-
-            @pl.when(k < z)
-            def _():
-                @pl.loop(0, 2)
-                def _(m):
-                    term(m, h, k)
-
-                    @pl.when(z == last)
-                    def _():
-                        for half in range(2):
-                            g_copy(m, h, k, 1, half).start()
-
-    def own_terms(h):
-        @pl.loop(0, 2)
-        def _(m):
-            term(m, h, z)
+    def term_step(m, h, i):
+        d = facing(i)
+        term(m, h, d)
+
+        @pl.when(((z == 0) | (z == last)) & (i < last))
+        def _():
+            for half in range(2):
+                g_copy(m, h, d, side, half).start()
 
     def add_rows(dst, dst_row, src, count, columns=slice(None)):
         step = math.gcd(count, 32)
@@ -581,8 +591,6 @@
             o = pl.multiple_of(i * step, step)
             at = pl.ds(pl.multiple_of(dst_row + o, math.gcd(step, 16)), step)
             dst[at, columns] = (dst[at, columns].astype(F32) + src[pl.ds(o, step), columns].astype(F32)).astype(BF16)
-
-    side = 2 * z // z_size
 
     def reduce_step(h, k, m, near):
         way = side if near else 1 - side
@@ -638,6 +646,11 @@
 
             (store_sum(m, h, x) if half else f_copy(m, h)).start()
 
+    def finish_at(h, m, ends):
+        @pl.when((z == 0) | (z == last) if ends else (z > 0) & (z < last))
+        def _():
+            finish(h, m)
+
     def finish_x(h, m):
         f_copy(m, h).wait_recv()
         step = math.gcd(blk, 32)
@@ -649,7 +662,6 @@
 
         store_sum(m, h, 1 - x).start()
 
-    span = 2 * blk
     tile = math.gcd(span, 256)
 
     def span_at(i):
@@ -675,21 +687,24 @@
         return remote(part.at[a, rows_at(q * chip_rows + (1 - c) * rows_dev, rows_dev), span_at(i)],
                       dbuf.at[a, q, :, span_at(i)], d_s.at[a], d_r.at[a, i], mate)
 
-    cut_q = rows_dev * 3 // 8 // 16 * 16
-    low, high = (0, cut_q), (cut_q, rows_dev - cut_q)
+    cuts_q = tuple(rows_dev * share // 8 // 16 * 16 for share in (2, 2))
     hops = (
-        (1 - x, y, low, qa, 0, x_next),
-        (1 - x, 1 - y, low, qa, 1, x_next),
-        (x, 1 - y, high, qb, 0, y_next),
-        (1 - x, 1 - y, high, qb, 1, y_next),
-        (x, 1 - y, low, qa, 2, y_next),
-        (1 - x, y, high, qb, 2, x_next),
+        (1 - x, y, 0, qa, 0, x_next),
+        (1 - x, 1 - y, 0, qa, 1, x_next),
+        (x, 1 - y, 1, qb, 0, y_next),
+        (1 - x, 1 - y, 1, qb, 1, y_next),
+        (x, 1 - y, 0, qa, 2, y_next),
+        (1 - x, y, 1, qb, 2, x_next),
     )
 
+    def bounds(a, high):
+        return (cuts_q[a], rows_dev - cuts_q[a]) if high else (0, cuts_q[a])
+
     def q_copy(a, k, i):
-        xx, yy, (lo, count), buf, slot, to = hops[k]
+        xx, yy, high, buf, slot, to = hops[k]
+        lo, count = bounds(a, high)
         return remote(part.at[a, rows_at(block_at(xx, yy, c) + lo, count), span_at(i)],
-                      buf.at[a, slot, :, span_at(i)], q_s.at[a], q_r.at[a, k // 2, i] if k in (1, 3) else q_l.at[a], to)
+                      buf.at[a, slot, pl.ds(0, count), span_at(i)], q_s.at[a], q_r.at[a, k // 2, i] if k in (1, 3) else q_l.at[a], to)
 
     def q_first(a, i):
         there = dbuf.at[a, :, :, span_at(i)]
@@ -705,10 +720,10 @@
 
     def q_second(a, i):
         q_copy(a, 1, i).wait_recv()
-        add_rows(part.at[a], block_at(x, 1 - y, c), qa.at[a, 1], cut_q, span_at(i))
+        add_rows(part.at[a], block_at(x, 1 - y, c), qa.at[a, 1], cuts_q[a], span_at(i))
         q_copy(a, 4, i).start()
         q_copy(a, 3, i).wait_recv()
-        add_rows(part.at[a], block_at(1 - x, y, c) + cut_q, qb.at[a, 1], rows_dev - cut_q, span_at(i))
+        add_rows(part.at[a], block_at(1 - x, y, c) + cuts_q[a], qb.at[a, 1], rows_dev - cuts_q[a], span_at(i))
         q_copy(a, 5, i).start()
 
     def over(lo, hi, *calls):
@@ -723,7 +738,8 @@
     def q_last(a):
         there = part.at[a, pl.ds(0, 2 * rows_dev), :]
         remote(there, there, q_s.at[a], q_l.at[a], x_next).wait_recv()
-        for (lo, count), buf in ((low, qa), (high, qb)):
+        for high, buf in enumerate((qa, qb)):
+            lo, count = bounds(a, high)
             step = math.gcd(count, 16)
 
             @pl.loop(0, count // step)
@@ -737,94 +753,132 @@
 
         store_out(a).start()
 
-    for m in range(2):
-        wx_copy(m, 0).start()
+    wx_copy(0, 0).start()
     for m in range(2):
         load_w(m, 0).wait()
         spread(m, 0, fs)
-    t_first(0)
-    t_first(1)
+    load_t(0).wait()
+    for u in range(z_size):
+        t_own(0, u)
+    wx_copy(1, 0).start()
+    from_x(0, (0,))
+    relay(0, 1, (0,), (0,))
+    t_pass(0, 0)
+    t_pass(0, 1)
+    relay(0, 1, (0,), (1,))
+    relay(0, 1, (1,), (0,))
+    t_pass(0, 2)
+    relay(0, 2, (0,), (0,))
+    t_pass(0, 3)
     for m in range(2):
         wx_copy(m, 1).start()
-    from_x(0)
-    relay(0, 1)
-    t_pass_y(0)
-    t_pass_x(0)
-    relay(0, 2)
-    t_pass_y(1)
-    t_pass_x(1)
+    load_t(1).wait()
+    t_own(1, 0)
+    t_own(1, 1)
+    t_diagonal(0, 0)
+    t_diagonal(0, 1)
+    relay(0, 2, (1,), (0,))
+    from_x(0, (1,))
+    relay(0, 2, (0,), (1,))
     for m in range(2):
         load_w(m, 1).wait()
-        spread(m, 1, fs)
-    t_first(2)
+        spread_at(m, 1, fs, True)
+    t_diagonal(0, 2)
+    t_diagonal(0, 3)
+    relay(0, 1, (1,), (1,))
+    settle(0, 0, 1, z_size)
+    t_mate(0)
+    earlier_hidden(0)
+    t_pass(1, 0)
+    t_own(1, 2)
+    relay(0, 2, (1,), (1,))
+    from_x_at(1, (0, 1), True)
+    spread_at(0, 1, fs, False)
+    from_x_at(1, (0,), False)
+    t_pass(1, 1)
+    t_own(1, 3)
+    t_diagonal(1, 0)
+    t_mate(1, 0)
+    term_step(1, 0, 0)
+    relay(1, 1, (0,), (0,))
+    t_pass(1, 2)
+    t_diagonal(1, 1)
+    t_mate(1, 1)
+    term_step(1, 0, 1)
+    relay(1, 1, (1,), (0,))
+    spread_at(1, 1, fs, False)
+    from_x_at(1, (1,), False)
+    t_pass(1, 3)
+    load_t(2).wait()
+    t_own(2)
+    t_diagonal(1, 2)
+    t_mate(1, 2)
+    term_step(1, 0, 2)
+    reduce_step(0, 0, 1, True)
+    t_diagonal(1, 3)
+    t_mate(1, 3)
+    settle(0, 1, 1, z_size)
+    earlier_pre_grad(0)
+    relay(1, 2, (0, 1), (0,))
+    over(0, z_size, lambda i: term_step(0, 0, i))
+    relay(1, 1, (0, 1), (1,))
+    reduce_step(0, 1, 1, True)
+    term_step(1, 0, last)
+    t_pass(2)
+    t_mate_blocks()
+    later_hidden(0, 0, 3)
+    settle(1, 0, 1, z_size)
+    later_hidden(1, 0, 3)
+    relay(1, 2, (0, 1), (1,))
+    reduce_step(0, 0, 1, False)
+    t_diagonal(2)
+    t_mate_diagonal()
+    for h in range(2):
+        later_hidden(h, 3, 4)
+    reduce_step(0, 0, 0, True)
+    settle(1, 1, 1, last)
+    partial(1, 2, 1, 0)
+    over(1, last, lambda i: partial(1, 2, 1, i), lambda i: q_first(1, i - 1), lambda i: q_rest(1, i - 1))
+    earlier_hidden(1)
+    q_first(1, last - 1)
+    q_rest(1, last - 1)
+    over(0, z_size, lambda i: term_step(1, 1, i))
+    q_second(1, 0)
     for m in range(2):
-        settle(0, m, 1, z_size)
-    for a in range(2):
-        t_mate(a)
-    earlier_hidden(0, 0, 3)
-    from_x(1)
-    t_diagonal(0)
-    relay(1, 1, (0,))
-    t_diagonal(1)
-    for a in range(2):
-        t_mate_diagonal(a)
-    earlier_hidden(0, 3, 4)
-    terms(0, 0, last)
-    own_terms(0)
-    relay(1, 1, (1,), (0,))
-    relay(1, 2, (0,), (0,))
-    t_pass_y(2)
-    reduce_step(0, 0, 0, True)
-    relay(1, 2, (1,), (0,))
-    relay(1, 1, (1,), (1,))
-    relay(1, 2, (0,), (1,))
-    t_pass_x(2)
-    reduce_step(0, 0, 1, True)
-    relay(1, 2, (1,), (1,))
-    reduce_step(0, 0, 0, False)
-    t_diagonal(2)
-    settle(1, 0, 1, z_size)
-    t_mate(2)
-    t_mate_diagonal(2)
-    later_hidden(0)
-    later_hidden(1)
+        totals[m].wait()
+    finish_at(0, 1, False)
     reduce_step(0, 1, 0, True)
-    reduce_step(0, 0, 1, False)
-    settle(1, 1, 1, last)
-    over(0, last, lambda i: partial(1, 2, 1, i))
     settle(1, 1, last, z_size)
     partial(1, 2, 1, last)
-    over(0, last, lambda i: q_first(1, i))
-    earlier_hidden(1, 0, 4)
-    reduce_step(0, 1, 1, True)
-    terms(1, 0, 1)
+    q_second(1, 1)
+    reduce_step(0, 0, 0, False)
+    earlier_pre_grad(1)
     q_first(1, last)
-    over(0, z_size, lambda i: q_rest(1, i))
-    terms(1, 1, last)
-    own_terms(1)
+    q_rest(1, last)
+    over(0, z_size, lambda i: term_step(0, 1, i))
+    q_second(1, 2)
+    finish_at(0, 1, True)
+    reduce_step(1, 0, 1, True)
     partial(0, 0, 0, 0)
     over(1, z_size, lambda i: partial(0, 0, 0, i), lambda i: q_first(0, i - 1))
-    for m in range(2):
-        totals[m].wait()
-        finish(0, m)
+    reduce_step(1, 1, 1, True)
+    q_second(1, last)
     q_first(0, last)
-    over(0, z_size, lambda i: q_second(1, i))
     over(0, z_size, lambda i: q_rest(0, i))
+    finish(0, 0)
+    reduce_step(1, 0, 1, False)
+    finish(1, 1)
     reduce_step(1, 0, 0, True)
-    reduce_step(1, 0, 1, True)
+    over(0, z_size, lambda i: q_second(0, i))
+    reduce_step(1, 1, 0, True)
     reduce_step(1, 0, 0, False)
-    over(0, z_size, lambda i: q_second(0, i))
+    finish_x(0, 1)
+    q_last(1)
+    finish(1, 0)
     finish_x(0, 0)
-    finish_x(0, 1)
-    reduce_step(1, 1, 0, True)
-    reduce_step(1, 0, 1, False)
-    reduce_step(1, 1, 1, True)
-    finish(1, 0)
-    q_last(1)
-    finish(1, 1)
+    finish_x(1, 1)
     q_last(0)
     finish_x(1, 0)
-    finish_x(1, 1)
 
     def sent(ref, semaphore):
         remote(ref, ref, semaphore, f_r.at[0, 0], mate).wait_send()
@@ -854,7 +908,7 @@
     blk, width = args[3].shape
     z_size, chunks, rows = n // 2, 2, rows_dev * 8
     cw = width // 2 // chunks
-    cut_q = rows_dev * 3 // 8 // 16 * 16
+    low, high = rows_dev * 2 // 8 // 16 * 16, rows_dev - rows_dev * 2 // 8 // 16 * 16
     dma = pltpu.SemaphoreType.DMA
     hbm = pl.BlockSpec(memory_space=pltpu.HBM)
     return pl.pallas_call(
@@ -870,6 +924,7 @@
         scratch_shapes=[
             pltpu.VMEM((3, rows, depth), BF16),
             pltpu.VMEM((2, chunks, depth, cw), BF16),
+            pltpu.VMEM((rows, cw), F32),
             pltpu.VMEM((3, chunks, rows, cw), BF16),
             pltpu.VMEM((2, chunks, depth, cw), BF16),
             pltpu.VMEM((2, chunks, z_size + 1, 2, blk, cw), BF16),
@@ -877,11 +932,11 @@
             pltpu.VMEM((2, chunks, blk, cw), BF16),
             pltpu.VMEM((2, rows, depth), BF16),
             pltpu.VMEM((2, 4, rows_dev, depth), BF16),
-            pltpu.VMEM((2, 3, cut_q, depth), BF16),
-            pltpu.VMEM((2, 3, rows_dev - cut_q, depth), BF16),
+            pltpu.VMEM((2, 3, low, depth), BF16),
+            pltpu.VMEM((2, 3, high, depth), BF16),
             pltpu.VMEM((2, rows_dev, depth), BF16),
             pltpu.VMEM((2, blk, width), F32),
-            dma((2 * chunks + 5,)), dma((4,)), dma((3,)), dma((3, 6)), dma, dma((2, 2, chunks)), dma((2, chunks, n)),
+            dma((2 * chunks + 5,)), dma((4,)), dma((3,)), dma((6 + 10 * z_size,)), dma, dma((2, 2, chunks)), dma((2, chunks, n)),
             dma((2, 2, chunks)), dma((2, chunks, z_size + 1, 2)), dma, dma((2, chunks)),
             dma((2,)), dma((2, z_size)), dma((2,)), dma((2, 2, z_size)), dma((2,)),
         ],

time: 129 us -> 123 us (0.953)
  Pallas kernels: 127 us -> 122 us
    pallas_call x1, Pallas kernels: 124 us -> 119 us  [plane_call(): pl.pallas_call(functools.partial(plane_kernel, n, chunks, factor), out_sh...]
where the time goes in v4:
time: 123 us
  Pallas kernels  122 us (99%)
    pallas_call x1, Pallas kernels, plane_call(): pl.pallas_call(functools.partial(plane_kernel, n, chunks, factor), out_sh...  119 us
    pallas_call x1, Pallas kernels, hand_on(): pl.pallas_call(hand_on_kernel, out_shape=tuple((jax.ShapeDtypeStruct(a.sh...  2.81 us

profile of v4, /device:TPU:0, one launch (start us, length us, event | category | flops | bytes accessed | tf_op | source)
XLA Modules:
  0.0 122.8 jit_solution(17878561523196431547)
XLA Ops:
  0.6 119.3 %feed_forward_planes.1 = (bf16[128,2048]{1,0:T(8,128)(2,1)}, bf16[128,2048]{1,0:T(8,128)(2,1)}, f32[256,1024]{1,0:T(8,128)}, f32[256,1024]{1,0:T(8,128)}) custom-call(bf16[128,2048]{1,0:T(8,128)(2,1)} %later_ref.1, bf16[128,2048]{1,0:T(8,128)(2,1)} %earlier_ref.1, bf16[128,2048]{1,0:T(8,128)(2,1)} %cot_ref.1, bf16[256,1024]{1,0:T(8,128)(2,1)} %up_ref.1, ...), custom_call_target="tpu_custom_call" | custom-call | tf_op jit(solution)/shard_map/feed_forward_planes/pallas_call | solution.py:914
  120.0 2.8 %feed_forward_results.1 = (bf16[128,2048]{1,0:T(8,128)(2,1)}, bf16[128,2048]{1,0:T(8,128)(2,1)}, f32[256,1024]{1,0:T(8,128)}, f32[256,1024]{1,0:T(8,128)}) custom-call(bf16[128,2048]{1,0:T(8,128)(2,1)} %get-tuple-element.8.refs_0_, bf16[128,2048]{1,0:T(8,128)(2,1)} %get-tuple-element.9.refs_1_, f32[256,1024]{1,0:T(8,128)} %get-tuple-element.10.refs_2_, ...), custom_call_target="tpu_custom_call" | custom-call | tf_op jit(solution)/shard_map/feed_forward_results/pallas_call | solution.py:972

commit v5 on v4

--- a/solution.py
+++ b/solution.py
@@ -475,15 +475,15 @@
 
     def moves(cut_t):
         return (
-            (x, y, 0, rows_dev, x_next, 0),
-            (x, y, 0, rows_dev, y_next, 1),
-            (1 - x, y, 0, cut_t, y_next, 2),
-            (x, 1 - y, cut_t, rows_dev - cut_t, x_next, 3),
-            (x, y, 0, rows_dev, mate, 4),
-            (1 - x, y, 0, rows_dev, mate, 4),
-            (x, 1 - y, 0, rows_dev, mate, 4),
-            (1 - x, 1 - y, 0, cut_t, mate, 5),
-            (1 - x, 1 - y, cut_t, rows_dev - cut_t, mate, 5),
+            (x, y, 0, rows_dev, x_next),
+            (x, y, 0, rows_dev, y_next),
+            (1 - x, y, 0, cut_t, y_next),
+            (x, 1 - y, cut_t, rows_dev - cut_t, x_next),
+            (x, y, 0, rows_dev, mate),
+            (1 - x, y, 0, rows_dev, mate),
+            (x, 1 - y, 0, rows_dev, mate),
+            (1 - x, 1 - y, 0, cut_t, mate),
+            (1 - x, 1 - y, cut_t, rows_dev - cut_t, mate),
         )
 
     cuts = tuple(rows_dev * part // 8 // 16 * 16 for part in (7, 5, 4))
@@ -492,24 +492,22 @@
         return (1 - side) * (last - i) + side * i
 
     def t_ref(a, start, count, u):
-        columns = slice(None) if u is None else rows_at(facing(u) * span, span)
-        return tok.at[a, rows_at(start, count), columns]
+        return tok.at[a, rows_at(start, count), slice(None) if u is None else rows_at(facing(u) * span, span)]
 
     def t_got(a, k, u):
-        if a == 2:
-            return t_r.at[moves(0)[k][-1]]
-        return t_r.at[6 + (a * 5 + min(k, 4)) * z_size + (0 if a == 0 and k > 3 else u)]
-
-    def t_copy(a, k, u=None):
-        xx, yy, lo, count, to, _ = moves(cuts[a])[k]
+        slot = u if k < 4 or a == 1 else k // 7 if a == 2 else 0
+        return t_r.at[a, min(k, 4), slot]
+
+    def t_copy(a, k, u):
+        xx, yy, lo, count, to = moves(cuts[a])[k]
         there = t_ref(a, block_at(xx, yy, c) + lo, count, u)
         return remote(there, there, t_s.at[a], t_got(a, k, u), to)
 
-    def t_own(a, u=None):
+    def t_own(a, u):
         for k in (0, 1, 4):
             t_copy(a, k, u).start()
 
-    def t_pass(a, u=None):
+    def t_pass(a, u):
         t_copy(a, 1, u).wait_recv()
         t_copy(a, 3, u).start()
         t_copy(a, 6, u).start()
@@ -517,7 +515,7 @@
         t_copy(a, 2, u).start()
         t_copy(a, 5, u).start()
 
-    def t_diagonal(a, u=None):
+    def t_diagonal(a, u):
         t_copy(a, 2, u).wait_recv()
         t_copy(a, 7, u).start()
         t_copy(a, 3, u).wait_recv()
@@ -529,11 +527,11 @@
 
     def t_mate_blocks():
         there = t_ref(2, 0, 3 * rows_dev, None)
-        remote(there, there, t_s.at[2], t_r.at[4], mate).wait_recv()
+        remote(there, there, t_s.at[2], t_got(2, 4, None), mate).wait_recv()
 
     def t_mate_diagonal():
         there = t_ref(2, 0, rows_dev, None)
-        remote(there, there, t_s.at[2], t_r.at[5], mate).wait_recv()
+        remote(there, there, t_s.at[2], t_got(2, 7, None), mate).wait_recv()
 
     def earlier_hidden(h):
         @pl.loop(0, 4)
@@ -687,7 +685,7 @@
         return remote(part.at[a, rows_at(q * chip_rows + (1 - c) * rows_dev, rows_dev), span_at(i)],
                       dbuf.at[a, q, :, span_at(i)], d_s.at[a], d_r.at[a, i], mate)
 
-    cuts_q = tuple(rows_dev * share // 8 // 16 * 16 for share in (2, 2))
+    cuts_q = tuple(rows_dev * share // 8 // 16 * 16 for share in (2, 3))
     hops = (
         (1 - x, y, 0, qa, 0, x_next),
         (1 - x, 1 - y, 0, qa, 1, x_next),
@@ -718,10 +716,12 @@
         for k in (0, 2):
             q_copy(a, k, i).start()
 
-    def q_second(a, i):
+    def q_second_y(a, i):
         q_copy(a, 1, i).wait_recv()
         add_rows(part.at[a], block_at(x, 1 - y, c), qa.at[a, 1], cuts_q[a], span_at(i))
         q_copy(a, 4, i).start()
+
+    def q_second_x(a, i):
         q_copy(a, 3, i).wait_recv()
         add_rows(part.at[a], block_at(1 - x, y, c) + cuts_q[a], qb.at[a, 1], rows_dev - cuts_q[a], span_at(i))
         q_copy(a, 5, i).start()
@@ -810,7 +810,8 @@
     from_x_at(1, (1,), False)
     t_pass(1, 3)
     load_t(2).wait()
-    t_own(2)
+    for u in range(z_size):
+        t_own(2, u)
     t_diagonal(1, 2)
     t_mate(1, 2)
     term_step(1, 0, 2)
@@ -819,57 +820,73 @@
     t_mate(1, 3)
     settle(0, 1, 1, z_size)
     earlier_pre_grad(0)
+    t_pass(2, 0)
     relay(1, 2, (0, 1), (0,))
     over(0, z_size, lambda i: term_step(0, 0, i))
+    t_pass(2, 1)
     relay(1, 1, (0, 1), (1,))
     reduce_step(0, 1, 1, True)
     term_step(1, 0, last)
-    t_pass(2)
+    t_pass(2, 2)
+    t_diagonal(2, 0)
+    t_pass(2, 3)
+    t_diagonal(2, 1)
     t_mate_blocks()
     later_hidden(0, 0, 3)
     settle(1, 0, 1, z_size)
     later_hidden(1, 0, 3)
     relay(1, 2, (0, 1), (1,))
     reduce_step(0, 0, 1, False)
-    t_diagonal(2)
+    t_diagonal(2, 2)
+    t_diagonal(2, 3)
     t_mate_diagonal()
     for h in range(2):
         later_hidden(h, 3, 4)
     reduce_step(0, 0, 0, True)
     settle(1, 1, 1, last)
     partial(1, 2, 1, 0)
-    over(1, last, lambda i: partial(1, 2, 1, i), lambda i: q_first(1, i - 1), lambda i: q_rest(1, i - 1))
+    partial(1, 2, 1, 1)
+    q_first(1, 0)
+    q_rest(1, 0)
     earlier_hidden(1)
-    q_first(1, last - 1)
-    q_rest(1, last - 1)
-    over(0, z_size, lambda i: term_step(1, 1, i))
-    q_second(1, 0)
+    q_first(1, 1)
+    q_rest(1, 1)
+    term_step(1, 1, 0)
+    over(2, last, lambda i: partial(1, 2, 1, i))
+    term_step(1, 1, 1)
+    q_first(1, 2)
+    over(2, z_size, lambda i: term_step(1, 1, i))
+    q_second_x(1, 0)
     for m in range(2):
         totals[m].wait()
     finish_at(0, 1, False)
     reduce_step(0, 1, 0, True)
     settle(1, 1, last, z_size)
     partial(1, 2, 1, last)
-    q_second(1, 1)
+    q_second_x(1, 1)
     reduce_step(0, 0, 0, False)
     earlier_pre_grad(1)
     q_first(1, last)
-    q_rest(1, last)
+    q_rest(1, 2)
     over(0, z_size, lambda i: term_step(0, 1, i))
-    q_second(1, 2)
+    q_second_x(1, 2)
     finish_at(0, 1, True)
     reduce_step(1, 0, 1, True)
     partial(0, 0, 0, 0)
     over(1, z_size, lambda i: partial(0, 0, 0, i), lambda i: q_first(0, i - 1))
     reduce_step(1, 1, 1, True)
-    q_second(1, last)
+    q_second_x(1, last)
     q_first(0, last)
+    q_rest(1, last)
+    over(0, z_size, lambda i: q_second_y(1, i))
     over(0, z_size, lambda i: q_rest(0, i))
     finish(0, 0)
     reduce_step(1, 0, 1, False)
+    over(0, last, lambda i: q_second_x(0, i))
     finish(1, 1)
     reduce_step(1, 0, 0, True)
-    over(0, z_size, lambda i: q_second(0, i))
+    q_second_x(0, last)
+    over(0, z_size, lambda i: q_second_y(0, i))
     reduce_step(1, 1, 0, True)
     reduce_step(1, 0, 0, False)
     finish_x(0, 1)
@@ -908,7 +925,7 @@
     blk, width = args[3].shape
     z_size, chunks, rows = n // 2, 2, rows_dev * 8
     cw = width // 2 // chunks
-    low, high = rows_dev * 2 // 8 // 16 * 16, rows_dev - rows_dev * 2 // 8 // 16 * 16
+    low, high = rows_dev * 3 // 8 // 16 * 16, rows_dev - rows_dev * 2 // 8 // 16 * 16
     dma = pltpu.SemaphoreType.DMA
     hbm = pl.BlockSpec(memory_space=pltpu.HBM)
     return pl.pallas_call(
@@ -936,7 +953,7 @@
             pltpu.VMEM((2, 3, high, depth), BF16),
             pltpu.VMEM((2, rows_dev, depth), BF16),
             pltpu.VMEM((2, blk, width), F32),
-            dma((2 * chunks + 5,)), dma((4,)), dma((3,)), dma((6 + 10 * z_size,)), dma, dma((2, 2, chunks)), dma((2, chunks, n)),
+            dma((2 * chunks + 5,)), dma((4,)), dma((3,)), dma((3, 5, z_size)), dma, dma((2, 2, chunks)), dma((2, chunks, n)),
             dma((2, 2, chunks)), dma((2, chunks, z_size + 1, 2)), dma, dma((2, chunks)),
             dma((2,)), dma((2, z_size)), dma((2,)), dma((2, 2, z_size)), dma((2,)),
         ],
@@ -956,14 +973,14 @@
         for i in range(2):
             o = pl.ds(i * half, half)
             loads.append(pltpu.make_async_copy(src.at[o, :], kept.at[o, :], in_s.at[a, i]))
-            stores.append(pltpu.make_async_copy(kept.at[o, :], dst.at[o, :], out_s.at[a, i]))
+            stores.append(pltpu.make_async_copy(kept.at[o, :], dst.at[o, :], out_s.at[a]))
     for load in loads:
         load.start()
     for load, store in zip(loads, stores):
         load.wait()
         store.start()
-    for store in stores:
-        store.wait()
+    for a, (kept, dst) in enumerate(zip(held, outs)):
+        pltpu.make_async_copy(kept, dst, out_s.at[a]).wait()
 
 
 def hand_on(*arrays):
@@ -975,7 +992,7 @@
         in_specs=[hbm] * count,
         out_specs=(hbm,) * count,
         scratch_shapes=[*(pltpu.VMEM(a.shape, a.dtype) for a in arrays),
-                        pltpu.SemaphoreType.DMA((count, 2)), pltpu.SemaphoreType.DMA((count, 2))],
+                        pltpu.SemaphoreType.DMA((count, 2)), pltpu.SemaphoreType.DMA((count,))],
         compiler_params=pltpu.CompilerParams(vmem_limit_bytes=67043328),
         name="feed_forward_results",
     )(*arrays)

time: 123 us -> 121 us (0.984)
    pallas_call x1, Pallas kernels: 119 us -> 118 us  [plane_call(): pl.pallas_call(functools.partial(plane_kernel, n, chunks, factor), out_sh...]
where the time goes in v5:
time: 121 us
  Pallas kernels  121 us (100%)
    pallas_call x1, Pallas kernels, plane_call(): pl.pallas_call(functools.partial(plane_kernel, n, chunks, factor), out_sh...  118 us
    pallas_call x1, Pallas kernels, hand_on(): pl.pallas_call(hand_on_kernel, out_shape=tuple((jax.ShapeDtypeStruct(a.sh...  2.78 us

profile of v5, /device:TPU:0, one launch (start us, length us, event | category | flops | bytes accessed | tf_op | source)
XLA Modules:
  0.0 121.2 jit_solution(15134050545642440148)
XLA Ops:
  0.6 117.8 %feed_forward_planes.1 = (bf16[128,2048]{1,0:T(8,128)(2,1)}, bf16[128,2048]{1,0:T(8,128)(2,1)}, f32[256,1024]{1,0:T(8,128)}, f32[256,1024]{1,0:T(8,128)}) custom-call(bf16[128,2048]{1,0:T(8,128)(2,1)} %later_ref.1, bf16[128,2048]{1,0:T(8,128)(2,1)} %earlier_ref.1, bf16[128,2048]{1,0:T(8,128)(2,1)} %cot_ref.1, bf16[256,1024]{1,0:T(8,128)(2,1)} %up_ref.1, ...), custom_call_target="tpu_custom_call" | custom-call | tf_op jit(solution)/shard_map/feed_forward_planes/pallas_call | solution.py:931
  118.4 2.8 %feed_forward_results.1 = (bf16[128,2048]{1,0:T(8,128)(2,1)}, bf16[128,2048]{1,0:T(8,128)(2,1)}, f32[256,1024]{1,0:T(8,128)}, f32[256,1024]{1,0:T(8,128)}) custom-call(bf16[128,2048]{1,0:T(8,128)(2,1)} %get-tuple-element.8.refs_0_, bf16[128,2048]{1,0:T(8,128)(2,1)} %get-tuple-element.9.refs_1_, f32[256,1024]{1,0:T(8,128)} %get-tuple-element.10.refs_2_, ...), custom_call_target="tpu_custom_call" | custom-call | tf_op jit(solution)/shard_map/feed_forward_results/pallas_call | solution.py:989

commit v6 on v5

--- a/solution.py
+++ b/solution.py
@@ -707,10 +707,12 @@
     def q_first(a, i):
         there = dbuf.at[a, :, :, span_at(i)]
         remote(there, there, d_s.at[a], d_r.at[a, i], mate).wait_recv()
-        for q in range(4):
-            add_rows(part.at[a], q * chip_rows + c * rows_dev, dbuf.at[a, q], rows_dev, span_at(i))
-        for k in (1, 3):
-            q_copy(a, k, i).start()
+        for chip in (3, 0, 1, 2):
+            start = chip_at(chip)
+            add_rows(part.at[a], start + c * rows_dev, dbuf.at[a, start // chip_rows], rows_dev, span_at(i))
+            if chip == 3:
+                for k in (1, 3):
+                    q_copy(a, k, i).start()
 
     def q_rest(a, i):
         for k in (0, 2):
@@ -857,6 +859,7 @@
     q_first(1, 2)
     over(2, z_size, lambda i: term_step(1, 1, i))
     q_second_x(1, 0)
+    q_second_y(1, 0)
     for m in range(2):
         totals[m].wait()
     finish_at(0, 1, False)
@@ -864,12 +867,14 @@
     settle(1, 1, last, z_size)
     partial(1, 2, 1, last)
     q_second_x(1, 1)
+    q_second_y(1, 1)
     reduce_step(0, 0, 0, False)
     earlier_pre_grad(1)
     q_first(1, last)
     q_rest(1, 2)
     over(0, z_size, lambda i: term_step(0, 1, i))
     q_second_x(1, 2)
+    q_second_y(1, 2)
     finish_at(0, 1, True)
     reduce_step(1, 0, 1, True)
     partial(0, 0, 0, 0)
@@ -878,7 +883,7 @@
     q_second_x(1, last)
     q_first(0, last)
     q_rest(1, last)
-    over(0, z_size, lambda i: q_second_y(1, i))
+    q_second_y(1, last)
     over(0, z_size, lambda i: q_rest(0, i))
     finish(0, 0)
     reduce_step(1, 0, 1, False)
@@ -974,11 +979,12 @@
             o = pl.ds(i * half, half)
             loads.append(pltpu.make_async_copy(src.at[o, :], kept.at[o, :], in_s.at[a, i]))
             stores.append(pltpu.make_async_copy(kept.at[o, :], dst.at[o, :], out_s.at[a]))
-    for load in loads:
-        load.start()
-    for load, store in zip(loads, stores):
-        load.wait()
-        store.start()
+    order = sorted(range(2 * count), key=lambda i: -i)
+    for i in order:
+        loads[i].start()
+    for i in order:
+        loads[i].wait()
+        stores[i].start()
     for a, (kept, dst) in enumerate(zip(held, outs)):
         pltpu.make_async_copy(kept, dst, out_s.at[a]).wait()
 

time: 121 us -> 121 us (level)
  no operation moved by 1% of the time
where the time goes in v6:
time: 121 us
  Pallas kernels  121 us (100%)
    pallas_call x1, Pallas kernels, plane_call(): pl.pallas_call(functools.partial(plane_kernel, n, chunks, factor), out_sh...  118 us
    pallas_call x1, Pallas kernels, hand_on(): pl.pallas_call(hand_on_kernel, out_shape=tuple((jax.ShapeDtypeStruct(a.sh...  2.8 us

profile of v6, /device:TPU:0, one launch (start us, length us, event | category | flops | bytes accessed | tf_op | source)
XLA Modules:
  0.0 121.2 jit_solution(4568385128865440085)
XLA Ops:
  0.6 117.8 %feed_forward_planes.1 = (bf16[128,2048]{1,0:T(8,128)(2,1)}, bf16[128,2048]{1,0:T(8,128)(2,1)}, f32[256,1024]{1,0:T(8,128)}, f32[256,1024]{1,0:T(8,128)}) custom-call(bf16[128,2048]{1,0:T(8,128)(2,1)} %later_ref.1, bf16[128,2048]{1,0:T(8,128)(2,1)} %earlier_ref.1, bf16[128,2048]{1,0:T(8,128)(2,1)} %cot_ref.1, bf16[256,1024]{1,0:T(8,128)(2,1)} %up_ref.1, ...), custom_call_target="tpu_custom_call" | custom-call | tf_op jit(solution)/shard_map/feed_forward_planes/pallas_call | solution.py:936
  118.4 2.8 %feed_forward_results.1 = (bf16[128,2048]{1,0:T(8,128)(2,1)}, bf16[128,2048]{1,0:T(8,128)(2,1)}, f32[256,1024]{1,0:T(8,128)}, f32[256,1024]{1,0:T(8,128)}) custom-call(bf16[128,2048]{1,0:T(8,128)(2,1)} %get-tuple-element.8.refs_0_, bf16[128,2048]{1,0:T(8,128)(2,1)} %get-tuple-element.9.refs_1_, f32[256,1024]{1,0:T(8,128)} %get-tuple-element.10.refs_2_, ...), custom_call_target="tpu_custom_call" | custom-call | tf_op jit(solution)/shard_map/feed_forward_results/pallas_call | solution.py:995

commit v7 on v5

--- a/solution.py
+++ b/solution.py
@@ -788,11 +788,11 @@
     relay(0, 1, (1,), (1,))
     settle(0, 0, 1, z_size)
     t_mate(0)
+    from_x_at(1, (0, 1), True)
     earlier_hidden(0)
     t_pass(1, 0)
     t_own(1, 2)
     relay(0, 2, (1,), (1,))
-    from_x_at(1, (0, 1), True)
     spread_at(0, 1, fs, False)
     from_x_at(1, (0,), False)
     t_pass(1, 1)

time: 121 us -> 121 us (level)
  no operation moved by 1% of the time
where the time goes in v7:
time: 121 us
  Pallas kernels  121 us (100%)
    pallas_call x1, Pallas kernels, plane_call(): pl.pallas_call(functools.partial(plane_kernel, n, chunks, factor), out_sh...  118 us
    pallas_call x1, Pallas kernels, hand_on(): pl.pallas_call(hand_on_kernel, out_shape=tuple((jax.ShapeDtypeStruct(a.sh...  2.78 us

profile of v7, /device:TPU:0, one launch (start us, length us, event | category | flops | bytes accessed | tf_op | source)
XLA Modules:
  0.0 121.2 jit_solution(11340351486359731979)
XLA Ops:
  0.6 117.8 %feed_forward_planes.1 = (bf16[128,2048]{1,0:T(8,128)(2,1)}, bf16[128,2048]{1,0:T(8,128)(2,1)}, f32[256,1024]{1,0:T(8,128)}, f32[256,1024]{1,0:T(8,128)}) custom-call(bf16[128,2048]{1,0:T(8,128)(2,1)} %later_ref.1, bf16[128,2048]{1,0:T(8,128)(2,1)} %earlier_ref.1, bf16[128,2048]{1,0:T(8,128)(2,1)} %cot_ref.1, bf16[256,1024]{1,0:T(8,128)(2,1)} %up_ref.1, ...), custom_call_target="tpu_custom_call" | custom-call | tf_op jit(solution)/shard_map/feed_forward_planes/pallas_call | solution.py:931
  118.4 2.8 %feed_forward_results.1 = (bf16[128,2048]{1,0:T(8,128)(2,1)}, bf16[128,2048]{1,0:T(8,128)(2,1)}, f32[256,1024]{1,0:T(8,128)}, f32[256,1024]{1,0:T(8,128)}) custom-call(bf16[128,2048]{1,0:T(8,128)(2,1)} %get-tuple-element.8.refs_0_, bf16[128,2048]{1,0:T(8,128)(2,1)} %get-tuple-element.9.refs_1_, f32[256,1024]{1,0:T(8,128)} %get-tuple-element.10.refs_2_, ...), custom_call_target="tpu_custom_call" | custom-call | tf_op jit(solution)/shard_map/feed_forward_results/pallas_call | solution.py:989
